TPU v7x, 128 devices: a 2x2x16 block of a 8x8x16 slice. The times are simulated.
128 devices in a mesh: grp: 4 (over y, x), ep: 32 (over z, core).
Axes of the slice: x: 2, y: 2, z: 16, core: 2. Of those that a mesh axis runs over, the one named last changes fastest.
The devices are a block of a 8x8x16 slice.
Arguments:
- tokens: bfloat16 [1024, 2048], P(('grp', 'ep')), parts along dimension 0, may hold values from -6 to 6
- state: float32 [1024, 8, 64, 128], P(('grp', 'ep')), parts along dimension 0, may hold values from -6 to 6
- g_mix: float32 [2048], replicated, may hold values from 0.1 to 1.9
- w_query: bfloat16 [2048, 512], P('ep'), may hold values from -0.125 to 0.125
- w_key: bfloat16 [2048, 512], P('ep'), may hold values from -0.125 to 0.125
- w_value: bfloat16 [2048, 1024], P('ep'), may hold values from -0.125 to 0.125
- w_decay_down: bfloat16 [2048, 32], replicated, may hold values from -0.125 to 0.125
- w_decay_up: bfloat16 [32, 512], replicated, may hold values from -1 to 1
- decay_bias: float32 [512], replicated, may hold values from -6 to 2
- g_head: float32 [128], replicated, may hold values from 0.1 to 1.9
- w_out: bfloat16 [1024, 2048], replicated, may hold values from -0.1875 to 0.1875
- g_ffn: float32 [2048], replicated, may hold values from 0.1 to 1.9
- routes: int32 [1024, 4], P(('grp', 'ep')), parts along dimension 0, may hold values from 0 to 31, all different within a row; in each aligned block of 8 rows (0 to 7, 8 to 15, ...) at most 2 rows name the same one
- route_scores: float32 [1024, 4], P(('grp', 'ep')), parts along dimension 0, may hold values from -9 to 320
- w_gate_in: bfloat16 [32, 2048, 1024], P('ep'), may hold values from -0.375 to 0.375
- w_lin_in: bfloat16 [32, 2048, 1024], P('ep'), may hold values from -0.375 to 0.375
- w_down: bfloat16 [32, 1024, 2048], P('ep'), may hold values from -0.046875 to 0.046875
Outputs:
- output: bfloat16 [1024, 2048], P(('grp', 'ep')), parts along dimension 0
- new_state: float32 [1024, 8, 64, 128], P(('grp', 'ep')), parts along dimension 0
There are 4 independent parts, one for each index of `grp`. A program takes and returns all parts, laid end to end along the dimension named above; an argument that names none is the same for every part. Nothing has to cross between parts.
Inputs may be any that keep to these rules, and one draw needn't show every extreme that they name: `routes`: each row names 4 different experts; the rows of one device name no expert more than 2 times, a bound that some block reaches.
All inputs are finite; a program needn't handle non-finite values.
Results may differ from a plain program's by a relative error of at most 0.014.
Values may be sent and summed in bfloat16 or wider, within the bound.
A program may use at most 128 MiB of HBM per device.

v0:
```python
import jax
import jax.numpy as jnp
from jax import lax
from jax.sharding import PartitionSpec as P

HEADS = 8
DK = 64
DV = 128
EXPERTS = 32
CAP = 2


EPS = 1e-06
TAU = 16.0
ALPHA = 1.702
LIMIT = 7.0


def in_one_piece(arrays, axis, dim, along):
    both = jnp.concatenate(arrays, axis=along)
    out, at, done = (lax.all_gather(both, axis, axis=dim, tiled=True), 0, [])
    for a in arrays:
        done.append(lax.slice_in_dim(out, at, at + a.shape[along], axis=along))
        at += a.shape[along]
    return tuple(done)


def rms_scale(values, gain):
    return values * lax.rsqrt(jnp.mean(values * values, axis=-1, keepdims=True) + EPS) * gain


def per_device(
    tokens,
    state,
    g_mix,
    w_query,
    w_key,
    w_value,
    w_decay_down,
    w_decay_up,
    decay_bias,
    g_head,
    w_out,
    g_ffn,
    routes,
    route_scores,
    w_gate_in,
    w_lin_in,
    w_down,
):
    seq_rows = tokens.shape[0]
    residual_in = tokens.astype(jnp.float32)
    normed = rms_scale(residual_in, g_mix).astype(jnp.bfloat16)
    pieces = in_one_piece((w_query, w_key, w_value), "ep", 0, 1)
    query_flat = jnp.dot(normed, pieces[0], preferred_element_type=jnp.float32)
    key_flat = jnp.dot(normed, pieces[1], preferred_element_type=jnp.float32)
    value_flat = jnp.dot(normed, pieces[2], preferred_element_type=jnp.float32)
    queries = query_flat.reshape(seq_rows, HEADS, DK) * DK ** (-0.5)
    key_rows = key_flat.reshape(seq_rows, HEADS, DK)
    value_rows = value_flat.reshape(seq_rows, HEADS, DV)
    low_rank = jnp.dot(normed, w_decay_down, preferred_element_type=jnp.float32).astype(
        jnp.bfloat16
    )
    log_decay = (
        jax.nn.log_sigmoid(
            jnp.dot(low_rank, w_decay_up, preferred_element_type=jnp.float32) + decay_bias
        )
        / TAU
    )
    log_decay = log_decay.reshape(seq_rows, HEADS, DK)
    new_state = (
        jnp.exp(log_decay)[..., None] * state + key_rows[..., None] * value_rows[:, :, None, :]
    )
    attended = jnp.einsum("bhk,bhkv->bhv", queries, new_state)
    headed = rms_scale(attended, g_head).astype(jnp.bfloat16).reshape(seq_rows, HEADS * DV)
    residual = (residual_in + jnp.dot(headed, w_out, preferred_element_type=jnp.float32)).astype(
        jnp.bfloat16
    )
    fed = rms_scale(residual.astype(jnp.float32), g_ffn).astype(jnp.bfloat16)
    top_count = routes.shape[1]
    slot_count = seq_rows * top_count
    slot_expert = routes.reshape(slot_count)
    slot_order = jnp.arange(slot_count, dtype=jnp.int32)
    earlier = (slot_expert[:, None] == slot_expert[None, :]) & (
        slot_order[None, :] < slot_order[:, None]
    )
    slot_rank = jnp.sum(earlier.astype(jnp.int32), axis=1)
    slot_dest = slot_expert * CAP + slot_rank
    slot_pick = (slot_dest[:, None] == jnp.arange(EXPERTS * CAP, dtype=jnp.int32)[None, :]).astype(
        jnp.bfloat16
    )
    token_pick = jnp.sum(slot_pick.reshape(seq_rows, top_count, EXPERTS * CAP), axis=1)
    outgoing = jnp.einsum("tx,td->xd", token_pick, fed, preferred_element_type=jnp.float32).astype(
        jnp.bfloat16
    )
    arrived = lax.all_to_all(outgoing, "ep", split_axis=0, concat_axis=0, tiled=True)
    local_experts = w_gate_in.shape[0]
    arrived = arrived.reshape(-1, local_experts, CAP, arrived.shape[1])
    gate_pre = jnp.minimum(
        jnp.einsum("secd,edf->secf", arrived, w_gate_in, preferred_element_type=jnp.float32), LIMIT
    )
    lin_pre = jnp.clip(
        jnp.einsum("secd,edf->secf", arrived, w_lin_in, preferred_element_type=jnp.float32),
        -LIMIT,
        LIMIT,
    )
    hidden = (gate_pre * jax.nn.sigmoid(ALPHA * gate_pre) * (lin_pre + 1.0)).astype(jnp.bfloat16)
    expert_out = jnp.einsum(
        "secf,efd->secd", hidden, w_down, preferred_element_type=jnp.float32
    ).astype(jnp.bfloat16)
    expert_out = expert_out.reshape(-1, expert_out.shape[3])
    returned = lax.all_to_all(expert_out, "ep", split_axis=0, concat_axis=0, tiled=True)
    gathered = jnp.einsum("sx,xd->sd", slot_pick, returned, preferred_element_type=jnp.float32)
    gathered = gathered.reshape(seq_rows, top_count, gathered.shape[1])
    weights = jax.nn.softmax(route_scores, axis=-1)
    expert_sum = jnp.sum(weights[..., None] * gathered, axis=1)
    output = (residual.astype(jnp.float32) + expert_sum).astype(jnp.bfloat16)
    return (output, new_state)


def solution(mesh):
    return jax.shard_map(
        per_device,
        mesh=mesh,
        in_specs=(
            P(("grp", "ep"), None),
            P(("grp", "ep"), None, None, None),
            P(),
            P("ep", None),
            P("ep", None),
            P("ep", None),
            P(),
            P(),
            P(),
            P(),
            P(),
            P(),
            P(("grp", "ep"), None),
            P(("grp", "ep"), None),
            P("ep", None, None),
            P("ep", None, None),
            P("ep", None, None),
        ),
        out_specs=(P(("grp", "ep"), None), P(("grp", "ep"), None, None, None)),
        check_vma=False,
    )
```

profile of v0, /device:TPU:69, one launch (start us, length us, event | category | flops | bytes accessed | tf_op | source)
XLA Modules:
  0.0 177.2 jit_solution(15484825665802088928)
XLA Ops:
  7.3 1.7 pad_maximum_fusion
  9.0 0.9 fusion.65
  9.9 1.2 fusion.73
  11.1 0.8 copy.38
  12.0 0.2 convert_reduce_fusion
  12.3 0.1 copy.40
  12.4 80.5 %all-gather.2.cloned.1.call-done = bf16[2048,2048]{1,0:T(8,128)(2,1)} async-done(((bf16[64,2048]{1,0:T(8,128)(2,1)}), bf16[2048,2048]{1,0:T(8,128)(2,1)}) %all-gather.2.cloned.1.call-update) | async-done | bytes 8388624 | tf_op jit(solution)/shard_map/all_gather | solution.py:21
  92.9 2.0 %fusion.45 = f32[8,512]{1,0:T(8,128)S(1)} fusion(bf16[2048,2048]{1,0:T(8,128)(2,1)} %all-gather.2.cloned.1.call-done, bf16[8,2048]{1,0:T(8,128)(2,1)} %param.17, f32[2048]{0:T(1024)} %param.19, f32[8]{0:T(128)S(1)} %add_rsqrt_fusion.2), kind=kOutput, calls=%fused_computation.29 | convolution fusion | flops 16846848 | bytes 2154528 | tf_op jit(solution)/shard_map/dot_general | solution.py:55
  95.0 2.9 %fusion.42 = f32[8,8,128]{2,0,1:T(8,128)S(1)} fusion(bf16[2048,2048]{1,0:T(8,128)(2,1)} %all-gather.2.cloned.1.call-done, bf16[8,2048]{1,0:T(8,128)(2,1)} %param.17, f32[2048]{0:T(1024)} %param.19, f32[8]{0:T(128)S(1)} %add_rsqrt_fusion.2), kind=kOutput, calls=%fused_computation.28 | convolution fusion | flops 33619968 | bytes 4268064 | tf_op jit(solution)/shard_map/dot_general | solution.py:57
  98.0 2.0 %fusion.13 = f32[8,512]{1,0:T(8,128)S(1)} fusion(bf16[2048,2048]{1,0:T(8,128)(2,1)} %all-gather.2.cloned.1.call-done, bf16[8,2048]{1,0:T(8,128)(2,1)S(1)} %copy-done.3, f32[2048]{0:T(1024)S(1)} %copy-done.4, f32[8]{0:T(128)S(1)} %add_rsqrt_fusion.2), kind=kOutput, calls=%fused_computation.14 | convolution fusion | flops 16842752 | bytes 2154528 | tf_op jit(solution)/shard_map/dot_general | solution.py:56
  100.1 2.6 %multiply_add_fusion = f32[8,8,64,128]{3,2,1,0:T(8,128)S(1)} fusion(f32[8,8,64,128]{3,2,1,0:T(8,128)} %param.18, f32[8,8,128]{2,1,0:T(8,128)S(1)} %copy.37, f32[8,8,64]{2,1,0:T(8,128)S(1)} %mul.131, f32[8,8,64]{2,1,0:T(8,128)S(1)} %exp.23), kind=kLoop, calls=%fused_computation.18 | loop fusion | flops 1572864 | bytes 4259840 | tf_op jit(solution)/shard_map/add | solution.py:72
  102.7 0.4 fusion.93
  103.3 0.8 multiply_reduce_fusion
  104.1 0.3 convolution_convert_fusion
  104.4 0.2 all_to_all.12
  104.6 29.9 %all_to_all.18 = bf16[32,2,2048]{2,1,0:T(2,128)(2,1)S(1)} all-to-all(bf16[32,2,2048]{2,1,0:T(2,128)(2,1)S(1)} %all_to_all.12), channel_id=1, replica_groups=mesh['grp'=4,'ep'=32] {'ep'}, dimensions={0} | all-to-all | bytes 524288 | tf_op jit(solution)/shard_map/all_to_all | solution.py:96
  134.5 3.0 %fusion.20 = f32[32,1,2,1024]{3,0,2,1:T(8,128)S(1)} fusion(bf16[1,2048,1024]{2,1,0:T(8,128)(2,1)} %param.31, bf16[32,2,2048]{2,1,0:T(2,128)(2,1)S(1)} %all_to_all.18), kind=kOutput, calls=%fused_computation.20 | convolution fusion | flops 268500992 | bytes 4718592 | tf_op jit(solution)/shard_map/secd,edf->secf/dot_general | solution.py:100
  137.5 5.1 %fusion.8 = bf16[32,2,2048]{2,0,1:T(8,128)(2,1)S(1)} fusion(bf16[1,1024,2048]{2,1,0:T(8,128)(2,1)} %param.33, bf16[1,2048,1024]{2,1,0:T(8,128)(2,1)} %param.32, f32[32,1,2,1024]{3,0,2,1:T(8,128)S(1)} %fusion.20, bf16[32,2,2048]{2,1,0:T(2,128)(2,1)S(1)} %all_to_all.18), kind=kOutput, calls=%fused_computation.9 | convolution fusion | flops 537591808 | bytes 9175040 | tf_op jit(solution)/shard_map/secf,efd->secd/dot_general | solution.py:108
  142.6 1.0 copy.44
  143.6 4.3 %all-to-all-start.1 = ((bf16[32,2,2048]{2,1,0:T(2,128)(2,1)}), bf16[32,2,2048]{2,1,0:T(2,128)(2,1)S(1)}, u32[]{:S(2)}, u32[]{:S(2)}) async-start(bf16[32,2,2048]{2,1,0:T(2,128)(2,1)} %copy.44), calls=%async_computation.1 | async-start | bytes 524288 | tf_op jit(solution)/shard_map/all_to_all | solution.py:112
  148.0 21.4 %all-to-all-done.1 = bf16[32,2,2048]{2,1,0:T(2,128)(2,1)S(1)} async-done(((bf16[32,2,2048]{2,1,0:T(2,128)(2,1)}), bf16[32,2,2048]{2,1,0:T(2,128)(2,1)S(1)}, u32[]{:S(2)}, u32[]{:S(2)}) %all-to-all-start.1) | async-done | bytes 262176 | tf_op jit(solution)/shard_map/all_to_all | solution.py:112
  169.4 0.1 reshape.139
  169.5 0.2 fusion.38
  169.7 0.6 add_convert_fusion
  (34 shorter events, 0.9 us)
Async XLA Ops:
  7.2 2.7 %copy-start = (bf16[2048,32]{0,1:T(8,128)(2,1)S(1)}, bf16[2048,32]{0,1:T(8,128)(2,1)}, u32[]{:S(2)}) copy-start(bf16[2048,32]{0,1:T(8,128)(2,1)} %param.23) | copy-start | bytes 393220
  7.2 90.8 %copy-start.3 = (bf16[8,2048]{1,0:T(8,128)(2,1)S(1)}, bf16[8,2048]{1,0:T(8,128)(2,1)}, u32[]{:S(2)}) copy-start(bf16[8,2048]{1,0:T(8,128)(2,1)} %param.17) | copy-start | bytes 98308
  7.2 90.8 %copy-start.4 = (f32[2048]{0:T(1024)S(1)}, f32[2048]{0:T(1024)}, u32[]{:S(2)}) copy-start(f32[2048]{0:T(1024)} %param.19) | copy-start | bytes 24580
  7.2 85.7 %all-gather.2.cloned.1.call-start = ((), (), s32[]{:S(2)}) async-start(), calls=%async_computation.2 | async-start | bytes 8650752 | tf_op jit(solution)/shard_map/all_gather | solution.py:21
  98.0 5.2 %copy-start.7 = (f32[128]{0:T(128)S(1)}, f32[128]{0:T(128)}, u32[]{:S(2)}) copy-start(f32[128]{0:T(128)} %param.26) | copy-start | bytes 1540
  100.1 3.2 %copy-start.2 = (bf16[1024,2048]{1,0:T(8,128)(2,1)S(1)}, bf16[1024,2048]{1,0:T(8,128)(2,1)}, u32[]{:S(2)}) copy-start(bf16[1024,2048]{1,0:T(8,128)(2,1)} %param.27) | copy-start | bytes 12582916
  102.7 34.8 %copy-start.1 = (f32[8,8,64,128]{3,2,1,0:T(8,128)}, f32[8,8,64,128]{3,2,1,0:T(8,128)S(1)}, u32[]{:S(2)}) copy-start(f32[8,8,64,128]{3,2,1,0:T(8,128)S(1)} %multiply_add_fusion) | copy-start | bytes 6291460
  102.7 1.4 copy-start.6
  137.5 10.4 %copy-start.5 = (f32[8,4]{0,1:T(4,128)S(1)}, f32[8,4]{0,1:T(4,128)}, u32[]{:S(2)}) copy-start(f32[8,4]{0,1:T(4,128)} %param.30) | copy-start | bytes 388
  143.6 25.8 %all-to-all-start.1 = ((bf16[32,2,2048]{2,1,0:T(2,128)(2,1)}), bf16[32,2,2048]{2,1,0:T(2,128)(2,1)S(1)}, u32[]{:S(2)}, u32[]{:S(2)}) async-start(bf16[32,2,2048]{2,1,0:T(2,128)(2,1)} %copy.44), calls=%async_computation.1 | async-start | bytes 524288 | tf_op jit(solution)/shard_map/all_to_all | solution.py:112
Sparse Core Ops, SparseCore 0:
  10.3 82.5 all-gather.1
where the time goes:
time: 178 us; the launch traced here: 177 us
  waiting for transfers between devices  102 us (57%)
  blocking collectives  29.9 us (17%)
  matrix products  17.9 us (10%)
  between operations  14.3 us (8%)
  other arithmetic  6.3 us (4%)
  starting transfers between devices  4.41 us (2%)
  local copies, waits for them, and re-layouts  2.54 us (1%)
    all_gather x1, waiting for transfers between devices, in_one_piece(): out, at, done = (lax.all_gather(both, axis, axis=dim, tiled=True), 0, [])  80.5 us
    all_to_all x1, blocking collectives, per_device(): lax.all_to_all(outgoing, 'ep', split_axis=0, concat_axis=0, tiled=True)  29.9 us
    all_to_all x1, waiting for transfers between devices, per_device(): lax.all_to_all(expert_out, 'ep', split_axis=0, concat_axis=0, tiled=True)  21.4 us
    dot_general x1, matrix products, per_device(): jnp.einsum('secf,efd->secd', hidden, w_down, preferred_element_type=jnp.f...  5.08 us
    all_to_all x1, starting transfers between devices, per_device(): lax.all_to_all(expert_out, 'ep', split_axis=0, concat_axis=0, tiled=True)  4.35 us
  transfers between devices with their start and end apart: 2, of which 2 were waited for; matrix products, arithmetic and copies ran while one was open for 2% of the time, Pallas kernels for 0%

commit v1 on v0

v1 whole, which is shorter than its diff:
```python
import functools

import jax
import jax.numpy as jnp
from jax import lax
from jax.experimental import pallas as pl
from jax.experimental.pallas import tpu as pltpu
from jax.sharding import PartitionSpec as P

MESH = pl.DeviceIdType.MESH
F32 = jnp.float32
BF16 = jnp.bfloat16

HEADS = 8
DK = 64
DV = 128
CAP = 2
EPS = 1e-06
TAU = 16.0
ALPHA = 1.702
LIMIT = 7.0

OFFSETS = (0, 3, -3, 6, -6, 8)
SEND_ORDER = (5, 3, 4, 1, 2, 0)


def rms(values, gain):
    return values * lax.rsqrt(jnp.mean(values * values, axis=-1, keepdims=True) + EPS) * gain


def dot(a, b, dims=None, precision=None):
    dims = dims or (((1,), (0,)), ((), ()))
    return lax.dot_general(a, b, dims, precision=precision, preferred_element_type=F32)


def iota(shape, dim):
    return lax.broadcasted_iota(jnp.int32, shape, dim)


def kernel(
    ep,
    tokens,
    g_mix,
    w_dd,
    w_du,
    d_bias,
    g_head,
    g_ffn,
    routes,
    scores,
    state,
    w_q,
    w_k,
    w_v,
    w_out,
    w_gate,
    w_lin,
    w_down,
    out,
    key_out,
    value_out,
    decay_out,
    own_w,
    st,
    wo,
    wg,
    wl,
    wd,
    xs,
    xbuf,
    wbuf,
    psend,
    rbuf,
    dsend,
    drecv,
    rsend,
    rrecv,
    xin,
    hid,
    eo,
    perm,
    perm_t,
    load_sems,
    send_sems,
    recv_sems,
):
    rows, width = tokens.shape
    chips = ep // 2
    me = lax.axis_index("ep")
    z, core = me // 2, lax.rem(me, 2)

    def wrap(i):
        return lax.rem(i + 2 * chips, chips)

    def dev(zz, cc):
        return {"ep": wrap(zz) * 2 + cc}

    barrier = pltpu.get_barrier_semaphore()

    def hello(i, carry):
        pl.semaphore_signal(
            barrier, inc=1, device_id={"ep": lax.rem(me + i, ep)}, device_id_type=MESH
        )
        return carry

    lax.fori_loop(1, ep, hello, 0)

    half = w_q.shape[1]
    loads = [
        pltpu.make_async_copy(w_q, own_w.at[0, :, pl.ds(0, half)], load_sems.at[0]),
        pltpu.make_async_copy(w_k, own_w.at[0, :, pl.ds(half, half)], load_sems.at[1]),
        pltpu.make_async_copy(w_v, own_w.at[1], load_sems.at[2]),
        pltpu.make_async_copy(state, st, load_sems.at[3]),
        pltpu.make_async_copy(w_out, wo, load_sems.at[4]),
        pltpu.make_async_copy(w_gate.at[0], wg, load_sems.at[5]),
        pltpu.make_async_copy(w_lin.at[0], wl, load_sems.at[6]),
        pltpu.make_async_copy(w_down.at[0], wd, load_sems.at[7]),
    ]
    for c in loads:
        c.start()

    tok = tokens[...].astype(F32)
    normed = rms(tok, g_mix[...]).astype(BF16)
    for i in range(chips + 2):
        j = (i - 1) % chips
        xs[i] = normed[:, 128 * j : 128 * (j + 1)]

    for c in loads[:3]:
        c.wait()

    pl.semaphore_wait(barrier, ep - 1)

    def copy(src, dst, phase, device):
        return pltpu.make_async_remote_copy(
            src_ref=src,
            dst_ref=dst,
            send_sem=send_sems.at[phase],
            recv_sem=recv_sems.at[phase],
            device_id=device,
            device_id_type=MESH,
        )

    for oi in SEND_ORDER[:-1]:
        o = OFFSETS[oi]
        zz = wrap(z + o)
        for cc in range(2):
            slot = 3 * (2 * oi + core)
            if o == 8:
                copy(
                    xs.at[pl.ds(zz + 1, 1)],
                    xbuf.at[pl.ds(slot + 1, 1)],
                    0,
                    dev(zz, cc),
                ).start()
            else:
                copy(
                    xs.at[pl.ds(zz, 3)], xbuf.at[pl.ds(slot, 3)], 0, dev(zz, cc)
                ).start()
    copy(xs.at[pl.ds(z, 3)], xbuf.at[pl.ds(3 * core, 3)], 0, dev(z, 1 - core)).start()
    for n in (1, -1):
        for cc in range(2):
            copy(own_w.at[cc], wbuf.at[2 * (1 - n) + core], 1, dev(z + n, cc)).start()
    copy(own_w.at[1 - core], wbuf.at[2 + core], 1, dev(z, 1 - core)).start()

    xbuf[pl.ds(3 * core, 3)] = xs[pl.ds(z, 3)]
    wbuf[2 + core] = own_w[core]
    for cc in range(2):
        empty = jnp.zeros(xbuf.shape[1:], BF16)
        xbuf[3 * (10 + cc)] = empty
        xbuf[3 * (10 + cc) + 2] = empty

    low_rank = dot(normed, w_dd[...], (((1,), (1,)), ((), ()))).astype(BF16)
    pre = dot(low_rank, w_du[...]) + d_bias[...]
    log_decay = (jnp.minimum(pre, 0.0) - jnp.log1p(jnp.exp(-jnp.abs(pre)))) / TAU
    decay = jnp.exp(log_decay)
    decay_out[...] = decay

    kbs = 8
    tall = kbs * rows
    wide = ep * CAP * kbs
    r_t = lax.rem(iota((tall, rows), 0), rows)
    spread = (r_t == iota((tall, rows), 1)).astype(F32)
    route_rows = dot(
        spread, routes[...].astype(F32), (((1,), (1,)), ((), ())), lax.Precision.HIGHEST
    )
    sc = scores[...]
    e_sc = jnp.exp(sc - jnp.max(sc, axis=0, keepdims=True))
    weights = e_sc / jnp.sum(e_sc, axis=0, keepdims=True)
    weight_rows = dot(spread, weights, (((1,), (1,)), ((), ())), lax.Precision.HIGHEST)
    col = iota((tall, wide), 1)
    row = iota((tall, wide), 0)
    col_e = (col // (CAP * kbs)).astype(F32)
    col_slot = (lax.rem(col, CAP * kbs) // kbs).astype(F32)
    has = jnp.zeros((tall, wide), F32)
    weighted = jnp.zeros((tall, wide), F32)
    for j in range(routes.shape[0]):
        hit = (route_rows[:, j : j + 1] == col_e).astype(F32)
        has += hit
        weighted += hit * weight_rows[:, j : j + 1]
    rr, rc = iota((tall, tall), 0), iota((tall, tall), 1)
    before = (rr // rows == rc // rows) & (rc < rr)
    rank = dot(before.astype(BF16), has.astype(BF16))
    pick = has * (rank == col_slot).astype(F32) * (row // rows == lax.rem(col, kbs)).astype(F32)
    combine = weighted * pick
    combine_hi = combine.astype(BF16)
    combine_lo = (combine - combine_hi.astype(F32)).astype(BF16)
    pick = pick.astype(BF16)

    p_r, p_c = iota((wide, wide), 0), iota((wide, wide), 1)
    slots = ep * CAP
    q = lax.rem(p_r, slots)
    perm[...] = (p_c == (q * kbs + p_r // slots)).astype(F32).astype(BF16)
    q = lax.rem(p_c, slots)
    perm_t[...] = (p_r == (q * kbs + p_c // slots)).astype(F32).astype(BF16)

    others = 2 * len(OFFSETS) - 1
    units = 3 * (others - 2) + 2
    pltpu.make_async_copy(
        xs.at[pl.ds(0, units)] if units <= xs.shape[0] else xbuf.at[pl.ds(0, units)],
        xbuf.at[pl.ds(0, units)],
        recv_sems.at[0],
    ).wait()
    pltpu.make_async_copy(
        wbuf.at[pl.ds(0, 5)], wbuf.at[pl.ds(0, 5)], recv_sems.at[1]
    ).wait()
    chunks = 2 * len(OFFSETS)
    cols = wbuf.shape[2]
    part = None
    for n in range(3):
        x = jnp.concatenate(
            [xbuf[3 * i + n].astype(F32) for i in range(chunks)], axis=0
        ).astype(BF16)
        w = wbuf[2 * n : 2 * n + 2].reshape(2 * wbuf.shape[1], cols)
        p = dot(x, w)
        part = p if part is None else part + p
    for i in range(chunks):
        one = part[rows * i : rows * (i + 1)]
        psend[i] = jnp.concatenate(
            [one[:, : cols // 2], one[:, cols // 2 :]], axis=0
        ).astype(BF16)
    for oi in SEND_ORDER[:-1]:
        o = OFFSETS[oi]
        for cc in range(2):
            copy(psend.at[2 * oi + cc], rbuf.at[2 * oi + core], 2, dev(z - o, cc)).start()
    copy(psend.at[1 - core], rbuf.at[core], 2, dev(z, 1 - core)).start()
    rbuf[core] = psend[core]
    pltpu.make_async_copy(
        psend.at[pl.ds(0, others)], rbuf.at[pl.ds(0, others)], recv_sems.at[2]
    ).wait()

    sums = []
    for h in range(2):
        total = rbuf[h].astype(F32)
        for oi in range(1, len(OFFSETS)):
            total += rbuf[2 * oi + h].astype(F32)
        sums.append(total)
    queries = sums[0][:rows] * DK ** (-0.5)
    keys = sums[0][rows:]
    values = jnp.concatenate([sums[1][:rows], sums[1][rows:]], axis=1)
    key_out[...] = keys
    value_out[...] = values

    loads[3].wait()
    qd = queries * decay
    qk = queries * keys
    block = iota((rows, rows * DK), 1) // DK == iota((rows, rows * DK), 0)
    gain = g_head[...]
    headed = []
    for h in range(HEADS):
        q_h = qd[:, DK * h : DK * (h + 1)]
        lhs = jnp.where(block, jnp.concatenate([q_h] * rows, axis=1), 0.0)
        s_h = st[:, h].reshape(rows * DK, DV)
        a_h = dot(lhs, s_h, precision=lax.Precision.HIGHEST)
        a_h += jnp.sum(qk[:, DK * h : DK * (h + 1)], axis=1, keepdims=True) * values[
            :, DV * h : DV * (h + 1)
        ]
        headed.append(rms(a_h, gain).astype(BF16))
    headed = jnp.concatenate(headed, axis=1)

    loads[4].wait()
    residual = (tok + dot(headed, wo[...])).astype(BF16).astype(F32)
    fed = rms(residual, g_ffn[...])

    lanes = width // kbs
    fed_rows = jnp.concatenate(
        [fed[:, lanes * k : lanes * (k + 1)] for k in range(kbs)], axis=0
    ).astype(BF16)
    dsend[...] = (
        dot(pick, fed_rows, (((0,), (0,)), ((), ()))).astype(BF16).reshape(dsend.shape)
    )

    def exchange(src, dst, phase):
        def to(zz, cc):
            there = wrap(zz) * 2 + cc
            copy(src.at[there], dst.at[me], phase, {"ep": there}).start()

        for cc in range(2):
            to(z + chips // 2, cc)

        def step(i, carry):
            d = chips // 2 - i
            for cc in range(2):
                to(z + d, cc)
                to(z - d, cc)
            return carry

        lax.fori_loop(1, chips // 2, step, 0)
        to(z, 1 - core)
        dst[me] = src[me]
        pltpu.make_async_copy(
            src.at[pl.ds(0, ep - 1)], dst.at[pl.ds(0, ep - 1)], recv_sems.at[phase]
        ).wait()

    exchange(dsend, drecv, 3)

    arrived = dot(perm[...], drecv[...].reshape(wide, lanes)).astype(BF16)
    for k in range(kbs):
        xin[:, lanes * k : lanes * (k + 1)] = arrived[slots * k : slots * (k + 1)]
    loads[5].wait()
    loads[6].wait()
    tile = 256

    def up(i, carry):
        at = pl.ds(pl.multiple_of(i * tile, tile), tile)
        x = xin[...]
        gate = jnp.minimum(dot(x, wg[:, at]), LIMIT)
        lin = jnp.clip(dot(x, wl[:, at]), -LIMIT, LIMIT)
        hid[:, at] = (gate * jax.nn.sigmoid(ALPHA * gate) * (lin + 1.0)).astype(BF16)
        return carry

    lax.fori_loop(0, wg.shape[1] // tile, up, 0)
    loads[7].wait()
    for k in range(kbs):
        eo[slots * k : slots * (k + 1)] = dot(
            hid[...], wd[:, lanes * k : lanes * (k + 1)]
        ).astype(BF16)
    rsend[...] = dot(perm_t[...], eo[...]).astype(BF16).reshape(rsend.shape)

    exchange(rsend, rrecv, 4)

    back = rrecv[...].reshape(wide, lanes)
    mixed = dot(combine_hi, back) + dot(combine_lo, back)
    for k in range(kbs):
        at = slice(lanes * k, lanes * (k + 1))
        out[:, at] = (residual[:, at] + mixed[rows * k : rows * (k + 1)]).astype(BF16)

    pltpu.make_async_copy(
        xbuf.at[pl.ds(0, units)], xbuf.at[pl.ds(0, units)], send_sems.at[0]
    ).wait()
    pltpu.make_async_copy(wbuf.at[pl.ds(0, 5)], wbuf.at[pl.ds(0, 5)], send_sems.at[1]).wait()
    pltpu.make_async_copy(
        psend.at[pl.ds(0, others)], rbuf.at[pl.ds(0, others)], send_sems.at[2]
    ).wait()
    for src, dst, phase in ((dsend, drecv, 3), (rsend, rrecv, 4)):
        pltpu.make_async_copy(
            src.at[pl.ds(0, ep - 1)], dst.at[pl.ds(0, ep - 1)], send_sems.at[phase]
        ).wait()


def per_device(
    ep,
    tokens,
    state,
    g_mix,
    w_query,
    w_key,
    w_value,
    w_decay_down,
    w_decay_up,
    decay_bias,
    g_head,
    w_out,
    g_ffn,
    routes,
    route_scores,
    w_gate_in,
    w_lin_in,
    w_down,
):
    rows, width = tokens.shape
    share, qk = w_query.shape
    vw = w_value.shape[1]
    ff = w_gate_in.shape[2]
    lanes = width // 8
    wide = ep * CAP * 8
    vmem = pl.BlockSpec(memory_space=pltpu.VMEM)
    hbm = pl.BlockSpec(memory_space=pl.ANY)
    chunks = 2 * len(OFFSETS)
    output, keys, values, decay = pl.pallas_call(
        functools.partial(kernel, ep),
        out_shape=(
            jax.ShapeDtypeStruct((rows, width), BF16),
            jax.ShapeDtypeStruct((rows, qk), F32),
            jax.ShapeDtypeStruct((rows, vw), F32),
            jax.ShapeDtypeStruct((rows, qk), F32),
        ),
        in_specs=[vmem] * 9 + [hbm] * 8,
        out_specs=(vmem,) * 4,
        scratch_shapes=[
            pltpu.VMEM((2, share, vw), BF16),
            pltpu.VMEM(state.shape, F32),
            pltpu.VMEM(w_out.shape, BF16),
            pltpu.VMEM(w_gate_in.shape[1:], BF16),
            pltpu.VMEM(w_lin_in.shape[1:], BF16),
            pltpu.VMEM(w_down.shape[1:], BF16),
            pltpu.VMEM((ep // 2 + 2, rows, 2 * share), BF16),
            pltpu.VMEM((3 * chunks, rows, 2 * share), BF16),
            pltpu.VMEM((6, share, vw), BF16),
            pltpu.VMEM((chunks, 2 * rows, vw // 2), BF16),
            pltpu.VMEM((chunks, 2 * rows, vw // 2), BF16),
            pltpu.VMEM((ep, CAP * 8, lanes), BF16),
            pltpu.VMEM((ep, CAP * 8, lanes), BF16),
            pltpu.VMEM((ep, CAP * 8, lanes), BF16),
            pltpu.VMEM((ep, CAP * 8, lanes), BF16),
            pltpu.VMEM((ep * CAP, width), BF16),
            pltpu.VMEM((ep * CAP, ff), BF16),
            pltpu.VMEM((wide, lanes), BF16),
            pltpu.VMEM((wide, wide), BF16),
            pltpu.VMEM((wide, wide), BF16),
            pltpu.SemaphoreType.DMA((8,)),
            pltpu.SemaphoreType.DMA((5,)),
            pltpu.SemaphoreType.DMA((5,)),
        ],
        compiler_params=pltpu.CompilerParams(
            collective_id=0, has_side_effects=True, vmem_limit_bytes=48 * 1024 * 1024
        ),
        name="layer",
    )(
        tokens,
        g_mix.reshape(1, width),
        w_decay_down.T,
        w_decay_up,
        decay_bias.reshape(1, qk),
        g_head.reshape(1, DV),
        g_ffn.reshape(1, width),
        routes.T,
        route_scores.T,
        state,
        w_query,
        w_key,
        w_value,
        w_out,
        w_gate_in,
        w_lin_in,
        w_down,
    )
    decay = decay.reshape(rows, HEADS, DK)
    keys = keys.reshape(rows, HEADS, DK)
    values = values.reshape(rows, HEADS, DV)
    new_state = decay[..., None] * state + keys[..., None] * values[:, :, None, :]
    return (output, new_state)


def solution(mesh):
    shard = P(("grp", "ep"), None)
    experts = P("ep", None, None)
    return jax.shard_map(
        functools.partial(per_device, mesh.shape["ep"]),
        mesh=mesh,
        in_specs=(
            shard,
            P(("grp", "ep"), None, None, None),
            P(),
            P("ep", None),
            P("ep", None),
            P("ep", None),
            P(),
            P(),
            P(),
            P(),
            P(),
            P(),
            shard,
            shard,
            experts,
            experts,
            experts,
        ),
        out_specs=(shard, P(("grp", "ep"), None, None, None)),
        check_vma=False,
    )
```

time: 178 us -> 86.6 us (0.49)
  waiting for transfers between devices: 102 us -> 0 us
  Pallas kernels: 0 us -> 71.7 us
  blocking collectives: 29.9 us -> 0 us
  matrix products: 17.9 us -> 0 us
  between operations: 14.3 us -> 0.68 us
  local copies, waits for them, and re-layouts: 2.54 us -> 11.5 us
  starting transfers between devices: 4.41 us -> 0 us
  other arithmetic: 6.3 us -> 2.21 us
    all_gather x1 -> x0, waiting for transfers between devices: 80.5 us -> none  [in_one_piece(): out, at, done = (lax.all_gather(both, axis, axis=dim, tiled=True), 0, [])]
    pallas_call x0 -> x1, Pallas kernels: none -> 71.7 us  [per_device(): pl.pallas_call(functools.partial(kernel, ep), out_shape=(jax.ShapeDtypeSt...]
    all_to_all x1 -> x0, blocking collectives: 29.9 us -> none  [per_device(): lax.all_to_all(outgoing, 'ep', split_axis=0, concat_axis=0, tiled=True)]
    all_to_all x1 -> x0, waiting for transfers between devices: 21.4 us -> none  [per_device(): lax.all_to_all(expert_out, 'ep', split_axis=0, concat_axis=0, tiled=True)]
    dot_general x10 -> x0, matrix products: 17.9 us -> none  [the longest x1 5.08 us: per_device(): jnp.einsum('secf,efd->secd', hidden, w_down, preferred_element_type=jnp.f...]
    unnamed x17 -> x29, local copies, waits for them, and re-layouts: 0.81 us -> 11.3 us
    all_to_all x1 -> x0, starting transfers between devices: 4.35 us -> none  [per_device(): lax.all_to_all(expert_out, 'ep', split_axis=0, concat_axis=0, tiled=True)]
  transfers between devices with their start and end apart: 2 -> 0, of which waited for: 2 -> 0; matrix products, arithmetic and copies ran while one was open for 2% -> 0% of each run, Pallas kernels for 0% -> 0%
where the time goes in v1:
time: 86.6 us; the launch traced here: 86 us
  Pallas kernels  71.7 us (83%)
  local copies, waits for them, and re-layouts  11.5 us (13%)
  other arithmetic  2.21 us (3%)
    pallas_call x1, Pallas kernels, per_device(): pl.pallas_call(functools.partial(kernel, ep), out_shape=(jax.ShapeDtypeSt...  71.7 us
    unnamed x29, local copies, waits for them, and re-layouts  11.3 us
    add x1, other arithmetic, per_device(): decay[..., None] * state + keys[..., None] * values[:, :, None, :]  2.21 us

profile of v1, /device:TPU:69, one launch (start us, length us, event | category | flops | bytes accessed | tf_op | source)
XLA Modules:
  0.0 86.0 jit_solution(6603843118319532091)
XLA Ops:
  0.6 0.0 copy-start
  0.6 1.6 %copy-done = f32[8,8,64,128]{3,2,1,0:T(8,128)S(1)} copy-done((f32[8,8,64,128]{3,2,1,0:T(8,128)S(1)}, f32[8,8,64,128]{3,2,1,0:T(8,128)}, u32[]{:S(2)}) %copy-start) | copy-done | bytes 2097176
  2.2 0.0 copy-start.2
  2.2 0.9 %copy-done.2 = bf16[2048,32]{0,1:T(8,128)(2,1)S(1)} copy-done((bf16[2048,32]{0,1:T(8,128)(2,1)S(1)}, bf16[2048,32]{0,1:T(8,128)(2,1)}, u32[]{:S(2)}) %copy-start.2) | copy-done | bytes 131096
  3.1 0.0 copy-start.3
  3.1 0.9 %copy-done.3 = bf16[64,1024]{1,0:T(8,128)(2,1)S(1)} copy-done((bf16[64,1024]{1,0:T(8,128)(2,1)S(1)}, bf16[64,1024]{1,0:T(8,128)(2,1)}, u32[]{:S(2)}) %copy-start.3) | copy-done | bytes 131096
  4.0 0.0 copy-start.4
  4.0 0.8 copy-done.4
  4.9 0.0 copy-start.5
  4.9 0.8 copy-done.5
  5.7 0.8 copy-done.6
  6.5 0.8 copy-done.7
  7.2 0.7 copy-done.8
  7.9 0.7 copy-done.9
  8.6 0.7 copy-done.10
  9.3 0.7 copy-done.11
  10.0 0.7 copy-done.12
  10.7 0.7 copy-done.13
  11.3 71.7 %layer.1 = (bf16[8,2048]{1,0:T(8,128)(2,1)S(1)}, f32[8,512]{1,0:T(8,128)S(1)}, f32[8,1024]{1,0:T(8,128)S(1)}, f32[8,512]{1,0:T(8,128)S(1)}) custom-call(bf16[8,2048]{1,0:T(8,128)(2,1)S(1)} %copy-done.6, f32[1,2048]{1,0:T(1,128)S(1)} %bitcast.10, bf16[32,2048]{1,0:T(8,128)(2,1)S(1)} %bitcast.8, bf16[32,512]{1,0:T(8,128)(2,1)S(1)} %copy-done.7, ...), custom_call_target="tpu_custom_call" | custom-call | tf_op jit(solution)/shard_map/layer/pallas_call | solution.py:389
  83.0 0.1 mul.27
  83.1 0.1 mul.30
  83.2 0.0 copy-done.1
  83.2 2.2 %multiply_add_fusion = f32[8,8,64,128]{3,2,1,0:T(8,128)} fusion(f32[8,8,64,128]{3,2,1,0:T(8,128)S(1)} %copy-done.1, f32[8,8,128]{2,1,0:T(8,128)S(1)} %copy.19, f32[8,8,64]{2,1,0:T(8,128)S(1)} %mul.30, f32[8,8,64]{2,1,0:T(8,128)S(1)} %mul.27), kind=kLoop, calls=%fused_computation | loop fusion | flops 1572864 | bytes 4259840 | tf_op jit(solution)/shard_map/add | solution.py:450
  85.4 0.6 copy.21
  (10 shorter events, 0.0 us)
Async XLA Ops:
  0.6 1.6 %copy-start = (f32[8,8,64,128]{3,2,1,0:T(8,128)S(1)}, f32[8,8,64,128]{3,2,1,0:T(8,128)}, u32[]{:S(2)}) copy-start(f32[8,8,64,128]{3,2,1,0:T(8,128)} %state.1) | copy-start | bytes 6291460
  2.2 0.9 %copy-start.2 = (bf16[2048,32]{0,1:T(8,128)(2,1)S(1)}, bf16[2048,32]{0,1:T(8,128)(2,1)}, u32[]{:S(2)}) copy-start(bf16[2048,32]{0,1:T(8,128)(2,1)} %param.23) | copy-start | bytes 393220
  3.1 0.9 %copy-start.3 = (bf16[64,1024]{1,0:T(8,128)(2,1)S(1)}, bf16[64,1024]{1,0:T(8,128)(2,1)}, u32[]{:S(2)}) copy-start(bf16[64,1024]{1,0:T(8,128)(2,1)} %w_v.1) | copy-start | bytes 393220
  4.0 0.8 copy-start.4
  4.9 0.8 copy-start.5
  5.7 0.8 copy-start.6
  6.5 0.8 copy-start.7
  7.2 0.7 copy-start.8
  7.9 0.7 copy-start.9
  8.6 0.7 copy-start.10
  9.3 0.7 copy-start.11
  10.0 0.7 copy-start.12
  10.7 0.7 copy-start.13
  11.3 71.9 %copy-start.1 = (f32[8,8,64,128]{3,2,1,0:T(8,128)S(1)}, f32[8,8,64,128]{3,2,1,0:T(8,128)}, u32[]{:S(2)}) copy-start(f32[8,8,64,128]{3,2,1,0:T(8,128)} %state.1) | copy-start | bytes 6291460

commit v2 on v1

--- a/solution.py
+++ b/solution.py
@@ -39,6 +39,25 @@
 
 def kernel(
     ep,
+    tokens_in,
+    g_mix_in,
+    w_dd_in,
+    w_du_in,
+    d_bias_in,
+    g_head_in,
+    g_ffn_in,
+    routes_in,
+    scores_in,
+    state,
+    w_q,
+    w_k,
+    w_v,
+    w_out,
+    w_gate,
+    w_lin,
+    w_down,
+    out,
+    state_out,
     tokens,
     g_mix,
     w_dd,
@@ -48,18 +67,6 @@
     g_ffn,
     routes,
     scores,
-    state,
-    w_q,
-    w_k,
-    w_v,
-    w_out,
-    w_gate,
-    w_lin,
-    w_down,
-    out,
-    key_out,
-    value_out,
-    decay_out,
     own_w,
     st,
     wo,
@@ -95,6 +102,32 @@
     def dev(zz, cc):
         return {"ep": wrap(zz) * 2 + cc}
 
+    half = w_q.shape[1]
+    pairs = [
+        (tokens_in, tokens),
+        (g_mix_in, g_mix),
+        (w_q, own_w.at[0, :, pl.ds(0, half)]),
+        (w_k, own_w.at[0, :, pl.ds(half, half)]),
+        (w_v, own_w.at[1]),
+        (w_dd_in, w_dd),
+        (w_du_in, w_du),
+        (d_bias_in, d_bias),
+        (routes_in, routes),
+        (scores_in, scores),
+        (g_head_in, g_head),
+        (g_ffn_in, g_ffn),
+        (state, st),
+        (w_out, wo),
+        (w_gate.at[0], wg),
+        (w_lin.at[0], wl),
+        (w_down.at[0], wd),
+    ]
+    loads = [
+        pltpu.make_async_copy(src, dst, load_sems.at[i]) for i, (src, dst) in enumerate(pairs)
+    ]
+    for c in loads[:5]:
+        c.start()
+
     barrier = pltpu.get_barrier_semaphore()
 
     def hello(i, carry):
@@ -103,21 +136,12 @@
         )
         return carry
 
-    lax.fori_loop(1, ep, hello, 0)
-
-    half = w_q.shape[1]
-    loads = [
-        pltpu.make_async_copy(w_q, own_w.at[0, :, pl.ds(0, half)], load_sems.at[0]),
-        pltpu.make_async_copy(w_k, own_w.at[0, :, pl.ds(half, half)], load_sems.at[1]),
-        pltpu.make_async_copy(w_v, own_w.at[1], load_sems.at[2]),
-        pltpu.make_async_copy(state, st, load_sems.at[3]),
-        pltpu.make_async_copy(w_out, wo, load_sems.at[4]),
-        pltpu.make_async_copy(w_gate.at[0], wg, load_sems.at[5]),
-        pltpu.make_async_copy(w_lin.at[0], wl, load_sems.at[6]),
-        pltpu.make_async_copy(w_down.at[0], wd, load_sems.at[7]),
-    ]
-    for c in loads:
-        c.start()
+    with jax.named_scope("hello"):
+        lax.fori_loop(1, ep, hello, 0)
+        for c in loads[5:]:
+            c.start()
+        for c in loads[:2]:
+            c.wait()
 
     tok = tokens[...].astype(F32)
     normed = rms(tok, g_mix[...]).astype(BF16)
@@ -125,10 +149,11 @@
         j = (i - 1) % chips
         xs[i] = normed[:, 128 * j : 128 * (j + 1)]
 
-    for c in loads[:3]:
+    for c in loads[2:5]:
         c.wait()
 
-    pl.semaphore_wait(barrier, ep - 1)
+    with jax.named_scope("barrier"):
+        pl.semaphore_wait(barrier, ep - 1)
 
     def copy(src, dst, phase, device):
         return pltpu.make_async_remote_copy(
@@ -169,11 +194,12 @@
         xbuf[3 * (10 + cc)] = empty
         xbuf[3 * (10 + cc) + 2] = empty
 
+    for c in loads[5:12]:
+        c.wait()
     low_rank = dot(normed, w_dd[...], (((1,), (1,)), ((), ()))).astype(BF16)
     pre = dot(low_rank, w_du[...]) + d_bias[...]
     log_decay = (jnp.minimum(pre, 0.0) - jnp.log1p(jnp.exp(-jnp.abs(pre)))) / TAU
     decay = jnp.exp(log_decay)
-    decay_out[...] = decay
 
     kbs = 8
     tall = kbs * rows
@@ -215,14 +241,14 @@
 
     others = 2 * len(OFFSETS) - 1
     units = 3 * (others - 2) + 2
-    pltpu.make_async_copy(
-        xs.at[pl.ds(0, units)] if units <= xs.shape[0] else xbuf.at[pl.ds(0, units)],
-        xbuf.at[pl.ds(0, units)],
-        recv_sems.at[0],
-    ).wait()
-    pltpu.make_async_copy(
-        wbuf.at[pl.ds(0, 5)], wbuf.at[pl.ds(0, 5)], recv_sems.at[1]
-    ).wait()
+    with jax.named_scope("tokens_wait"):
+        pltpu.make_async_copy(
+            xbuf.at[pl.ds(0, units)], xbuf.at[pl.ds(0, units)], recv_sems.at[0]
+        ).wait()
+    with jax.named_scope("weights_wait"):
+        pltpu.make_async_copy(
+            wbuf.at[pl.ds(0, 5)], wbuf.at[pl.ds(0, 5)], recv_sems.at[1]
+        ).wait()
     chunks = 2 * len(OFFSETS)
     cols = wbuf.shape[2]
     part = None
@@ -244,9 +270,10 @@
             copy(psend.at[2 * oi + cc], rbuf.at[2 * oi + core], 2, dev(z - o, cc)).start()
     copy(psend.at[1 - core], rbuf.at[core], 2, dev(z, 1 - core)).start()
     rbuf[core] = psend[core]
-    pltpu.make_async_copy(
-        psend.at[pl.ds(0, others)], rbuf.at[pl.ds(0, others)], recv_sems.at[2]
-    ).wait()
+    with jax.named_scope("partials_wait"):
+        pltpu.make_async_copy(
+            psend.at[pl.ds(0, others)], rbuf.at[pl.ds(0, others)], recv_sems.at[2]
+        ).wait()
 
     sums = []
     for h in range(2):
@@ -257,10 +284,8 @@
     queries = sums[0][:rows] * DK ** (-0.5)
     keys = sums[0][rows:]
     values = jnp.concatenate([sums[1][:rows], sums[1][rows:]], axis=1)
-    key_out[...] = keys
-    value_out[...] = values
-
-    loads[3].wait()
+
+    loads[12].wait()
     qd = queries * decay
     qk = queries * keys
     block = iota((rows, rows * DK), 1) // DK == iota((rows, rows * DK), 0)
@@ -277,7 +302,7 @@
         headed.append(rms(a_h, gain).astype(BF16))
     headed = jnp.concatenate(headed, axis=1)
 
-    loads[4].wait()
+    loads[13].wait()
     residual = (tok + dot(headed, wo[...])).astype(BF16).astype(F32)
     fed = rms(residual, g_ffn[...])
 
@@ -307,17 +332,36 @@
         lax.fori_loop(1, chips // 2, step, 0)
         to(z, 1 - core)
         dst[me] = src[me]
+
+    def arrive(src, dst, phase):
         pltpu.make_async_copy(
             src.at[pl.ds(0, ep - 1)], dst.at[pl.ds(0, ep - 1)], recv_sems.at[phase]
         ).wait()
 
-    exchange(dsend, drecv, 3)
+    with jax.named_scope("dispatch"):
+        exchange(dsend, drecv, 3)
+
+    with jax.named_scope("new_state"):
+        decay_cols, key_cols = decay.T, keys.T
+        for t in range(rows):
+            for h in range(HEADS):
+                at = slice(DK * h, DK * (h + 1))
+                st[t, h] = (
+                    decay_cols[at, t : t + 1] * st[t, h]
+                    + key_cols[at, t : t + 1] * values[t : t + 1, DV * h : DV * (h + 1)]
+                )
+
+        store = pltpu.make_async_copy(st, state_out, load_sems.at[12])
+        store.start()
+
+    with jax.named_scope("dispatch_wait"):
+        arrive(dsend, drecv, 3)
 
     arrived = dot(perm[...], drecv[...].reshape(wide, lanes)).astype(BF16)
     for k in range(kbs):
         xin[:, lanes * k : lanes * (k + 1)] = arrived[slots * k : slots * (k + 1)]
-    loads[5].wait()
-    loads[6].wait()
+    loads[14].wait()
+    loads[15].wait()
     tile = 256
 
     def up(i, carry):
@@ -329,14 +373,17 @@
         return carry
 
     lax.fori_loop(0, wg.shape[1] // tile, up, 0)
-    loads[7].wait()
+    loads[16].wait()
     for k in range(kbs):
         eo[slots * k : slots * (k + 1)] = dot(
             hid[...], wd[:, lanes * k : lanes * (k + 1)]
         ).astype(BF16)
     rsend[...] = dot(perm_t[...], eo[...]).astype(BF16).reshape(rsend.shape)
 
-    exchange(rsend, rrecv, 4)
+    with jax.named_scope("back"):
+        exchange(rsend, rrecv, 4)
+    with jax.named_scope("back_wait"):
+        arrive(rsend, rrecv, 4)
 
     back = rrecv[...].reshape(wide, lanes)
     mixed = dot(combine_hi, back) + dot(combine_lo, back)
@@ -344,6 +391,7 @@
         at = slice(lanes * k, lanes * (k + 1))
         out[:, at] = (residual[:, at] + mixed[rows * k : rows * (k + 1)]).astype(BF16)
 
+    store.wait()
     pltpu.make_async_copy(
         xbuf.at[pl.ds(0, units)], xbuf.at[pl.ds(0, units)], send_sems.at[0]
     ).wait()
@@ -384,19 +432,26 @@
     lanes = width // 8
     wide = ep * CAP * 8
     vmem = pl.BlockSpec(memory_space=pltpu.VMEM)
-    hbm = pl.BlockSpec(memory_space=pl.ANY)
+    hbm = pl.BlockSpec(memory_space=pltpu.HBM)
     chunks = 2 * len(OFFSETS)
-    output, keys, values, decay = pl.pallas_call(
+    return pl.pallas_call(
         functools.partial(kernel, ep),
         out_shape=(
             jax.ShapeDtypeStruct((rows, width), BF16),
-            jax.ShapeDtypeStruct((rows, qk), F32),
-            jax.ShapeDtypeStruct((rows, vw), F32),
-            jax.ShapeDtypeStruct((rows, qk), F32),
+            jax.ShapeDtypeStruct(state.shape, F32),
         ),
-        in_specs=[vmem] * 9 + [hbm] * 8,
-        out_specs=(vmem,) * 4,
+        in_specs=[hbm] * 17,
+        out_specs=(vmem, hbm),
         scratch_shapes=[
+            pltpu.VMEM((rows, width), BF16),
+            pltpu.VMEM((1, width), F32),
+            pltpu.VMEM(w_decay_down.shape[::-1], BF16),
+            pltpu.VMEM(w_decay_up.shape, BF16),
+            pltpu.VMEM((1, qk), F32),
+            pltpu.VMEM((1, DV), F32),
+            pltpu.VMEM((1, width), F32),
+            pltpu.VMEM(routes.shape[::-1], jnp.int32),
+            pltpu.VMEM(route_scores.shape[::-1], F32),
             pltpu.VMEM((2, share, vw), BF16),
             pltpu.VMEM(state.shape, F32),
             pltpu.VMEM(w_out.shape, BF16),
@@ -417,12 +472,12 @@
             pltpu.VMEM((wide, lanes), BF16),
             pltpu.VMEM((wide, wide), BF16),
             pltpu.VMEM((wide, wide), BF16),
-            pltpu.SemaphoreType.DMA((8,)),
+            pltpu.SemaphoreType.DMA((17,)),
             pltpu.SemaphoreType.DMA((5,)),
             pltpu.SemaphoreType.DMA((5,)),
         ],
         compiler_params=pltpu.CompilerParams(
-            collective_id=0, has_side_effects=True, vmem_limit_bytes=48 * 1024 * 1024
+            collective_id=0, has_side_effects=True, vmem_limit_bytes=63_000_000
         ),
         name="layer",
     )(
@@ -444,11 +499,6 @@
         w_lin_in,
         w_down,
     )
-    decay = decay.reshape(rows, HEADS, DK)
-    keys = keys.reshape(rows, HEADS, DK)
-    values = values.reshape(rows, HEADS, DV)
-    new_state = decay[..., None] * state + keys[..., None] * values[:, :, None, :]
-    return (output, new_state)
 
 
 def solution(mesh):

time: 86.6 us -> 78.6 us (0.908)
  local copies, waits for them, and re-layouts: 11.5 us -> 4.53 us
  other arithmetic: 2.21 us -> 0 us
  Pallas kernels: 71.7 us -> 73.2 us
    unnamed x29 -> x2, local copies, waits for them, and re-layouts: 11.3 us -> 4.53 us
    add x1 -> x0, other arithmetic: 2.21 us -> none  [per_device(): decay[..., None] * state + keys[..., None] * values[:, :, None, :]]
    pallas_call x1, Pallas kernels: 71.7 us -> 73.2 us  [per_device(): pl.pallas_call(functools.partial(kernel, ep), out_shape=(jax.ShapeDtypeSt...]
where the time goes in v2:
time: 78.6 us; the launch traced here: 78.4 us
  Pallas kernels  73.2 us (93%)
  local copies, waits for them, and re-layouts  4.53 us (6%)
    pallas_call x1, Pallas kernels, per_device(): pl.pallas_call(functools.partial(kernel, ep), out_shape=(jax.ShapeDtypeSt...  73.2 us
    unnamed x2, local copies, waits for them, and re-layouts  4.53 us

profile of v2, /device:TPU:69, one launch (start us, length us, event | category | flops | bytes accessed | tf_op | source)
XLA Modules:
  0.0 78.4 jit_solution(4768572147837675251)
XLA Ops:
  0.6 73.2 %layer.1 = (bf16[8,2048]{1,0:T(8,128)(2,1)}, f32[8,8,64,128]{3,2,1,0:T(8,128)}) custom-call(bf16[8,2048]{1,0:T(8,128)(2,1)} %tokens_in.1, f32[1,2048]{1,0:T(1,128)} %bitcast.8, bf16[32,2048]{1,0:T(8,128)(2,1)} %bitcast.7, bf16[32,512]{1,0:T(8,128)(2,1)} %w_du_in.1, f32[1,512]{1,0:T(1,128)} %bitcast.10, f32[1,128]{1,0:T(1,128)} %bitcast.13, ...), custom_call_target="tpu_custom_call" | custom-call | tf_op jit(solution)/shard_map/layer/pallas_call | solution.py:437
  73.9 1.4 %copy.21 = bf16[8,2048]{1,0:T(8,128)(2,1)} copy(bf16[8,2048]{1,0:T(8,128)(2,1)} %get-tuple-element.4) | data formatting | bytes 65536
  75.2 3.2 %copy.22 = f32[8,8,64,128]{3,2,1,0:T(8,128)} copy(f32[8,8,64,128]{3,2,1,0:T(8,128)} %get-tuple-element.5) | data formatting | bytes 4194304

commit v3 on v2

--- a/solution.py
+++ b/solution.py
@@ -20,8 +20,9 @@
 ALPHA = 1.702
 LIMIT = 7.0
 
-OFFSETS = (0, 3, -3, 6, -6, 8)
-SEND_ORDER = (5, 3, 4, 1, 2, 0)
+OFFSETS = (1, 4, 7, -2, -5, -7)
+SEND_ORDER = (2, 5, 4, 1, 3, 0)
+RING = (8, 7, -7, 6, -6, 5, -5, 4, -4, 3, -3, 2, -2, 1, -1, 0)
 
 
 def rms(values, gain):
@@ -165,29 +166,20 @@
             device_id_type=MESH,
         )
 
-    for oi in SEND_ORDER[:-1]:
-        o = OFFSETS[oi]
-        zz = wrap(z + o)
+    for oi in SEND_ORDER:
         for cc in range(2):
+            zz = wrap(z + (1 - 2 * cc) * OFFSETS[oi])
             slot = 3 * (2 * oi + core)
-            if o == 8:
-                copy(
-                    xs.at[pl.ds(zz + 1, 1)],
-                    xbuf.at[pl.ds(slot + 1, 1)],
-                    0,
-                    dev(zz, cc),
-                ).start()
+            if oi == len(OFFSETS) - 1:
+                src, dst = xs.at[pl.ds(zz + 1, 1)], xbuf.at[pl.ds(slot + 1, 1)]
             else:
-                copy(
-                    xs.at[pl.ds(zz, 3)], xbuf.at[pl.ds(slot, 3)], 0, dev(zz, cc)
-                ).start()
-    copy(xs.at[pl.ds(z, 3)], xbuf.at[pl.ds(3 * core, 3)], 0, dev(z, 1 - core)).start()
+                src, dst = xs.at[pl.ds(zz, 3)], xbuf.at[pl.ds(slot, 3)]
+            copy(src, dst, 0, dev(zz, cc)).start()
     for n in (1, -1):
         for cc in range(2):
             copy(own_w.at[cc], wbuf.at[2 * (1 - n) + core], 1, dev(z + n, cc)).start()
     copy(own_w.at[1 - core], wbuf.at[2 + core], 1, dev(z, 1 - core)).start()
 
-    xbuf[pl.ds(3 * core, 3)] = xs[pl.ds(z, 3)]
     wbuf[2 + core] = own_w[core]
     for cc in range(2):
         empty = jnp.zeros(xbuf.shape[1:], BF16)
@@ -232,15 +224,14 @@
     combine_lo = (combine - combine_hi.astype(F32)).astype(BF16)
     pick = pick.astype(BF16)
 
-    p_r, p_c = iota((wide, wide), 0), iota((wide, wide), 1)
-    slots = ep * CAP
-    q = lax.rem(p_r, slots)
-    perm[...] = (p_c == (q * kbs + p_r // slots)).astype(F32).astype(BF16)
-    q = lax.rem(p_c, slots)
-    perm_t[...] = (p_r == (q * kbs + p_c // slots)).astype(F32).astype(BF16)
-
-    others = 2 * len(OFFSETS) - 1
-    units = 3 * (others - 2) + 2
+    part_rows = wide // 2
+    slots = part_rows // kbs
+    p_r, p_c = iota((part_rows, part_rows), 0), iota((part_rows, part_rows), 1)
+    perm[...] = (p_c == (lax.rem(p_r, slots) * kbs + p_r // slots)).astype(F32).astype(BF16)
+    perm_t[...] = (p_r == (lax.rem(p_c, slots) * kbs + p_c // slots)).astype(F32).astype(BF16)
+
+    chunks = 2 * len(OFFSETS)
+    units = 3 * (chunks - 2) + 2
     with jax.named_scope("tokens_wait"):
         pltpu.make_async_copy(
             xbuf.at[pl.ds(0, units)], xbuf.at[pl.ds(0, units)], recv_sems.at[0]
@@ -249,7 +240,6 @@
         pltpu.make_async_copy(
             wbuf.at[pl.ds(0, 5)], wbuf.at[pl.ds(0, 5)], recv_sems.at[1]
         ).wait()
-    chunks = 2 * len(OFFSETS)
     cols = wbuf.shape[2]
     part = None
     for n in range(3):
@@ -264,15 +254,14 @@
         psend[i] = jnp.concatenate(
             [one[:, : cols // 2], one[:, cols // 2 :]], axis=0
         ).astype(BF16)
-    for oi in SEND_ORDER[:-1]:
-        o = OFFSETS[oi]
+    sign = 1 - 2 * core
+    for oi in SEND_ORDER:
         for cc in range(2):
-            copy(psend.at[2 * oi + cc], rbuf.at[2 * oi + core], 2, dev(z - o, cc)).start()
-    copy(psend.at[1 - core], rbuf.at[core], 2, dev(z, 1 - core)).start()
-    rbuf[core] = psend[core]
+            to = dev(z - sign * OFFSETS[oi], cc)
+            copy(psend.at[2 * oi + cc], rbuf.at[2 * oi + core], 2, to).start()
     with jax.named_scope("partials_wait"):
         pltpu.make_async_copy(
-            psend.at[pl.ds(0, others)], rbuf.at[pl.ds(0, others)], recv_sems.at[2]
+            psend, rbuf, recv_sems.at[2]
         ).wait()
 
     sums = []
@@ -314,32 +303,17 @@
         dot(pick, fed_rows, (((0,), (0,)), ((), ()))).astype(BF16).reshape(dsend.shape)
     )
 
-    def exchange(src, dst, phase):
-        def to(zz, cc):
-            there = wrap(zz) * 2 + cc
-            copy(src.at[there], dst.at[me], phase, {"ep": there}).start()
-
-        for cc in range(2):
-            to(z + chips // 2, cc)
-
-        def step(i, carry):
-            d = chips // 2 - i
+    with jax.named_scope("dispatch"):
+        for j, o in enumerate(RING):
             for cc in range(2):
-                to(z + d, cc)
-                to(z - d, cc)
-            return carry
-
-        lax.fori_loop(1, chips // 2, step, 0)
-        to(z, 1 - core)
-        dst[me] = src[me]
-
-    def arrive(src, dst, phase):
-        pltpu.make_async_copy(
-            src.at[pl.ds(0, ep - 1)], dst.at[pl.ds(0, ep - 1)], recv_sems.at[phase]
-        ).wait()
-
-    with jax.named_scope("dispatch"):
-        exchange(dsend, drecv, 3)
+                there = wrap(z + o) * 2 + cc
+                if o:
+                    copy(
+                        dsend.at[there], drecv.at[2 * j + core], 3 + j // (ep // 4), {"ep": there}
+                    ).start()
+        there = 2 * z + 1 - core
+        copy(dsend.at[there], drecv.at[ep - 2 + core], 4, {"ep": there}).start()
+        drecv[ep - 2 + core] = dsend[me]
 
     with jax.named_scope("new_state"):
         decay_cols, key_cols = decay.T, keys.T
@@ -354,36 +328,63 @@
         store = pltpu.make_async_copy(st, state_out, load_sems.at[12])
         store.start()
 
-    with jax.named_scope("dispatch_wait"):
-        arrive(dsend, drecv, 3)
-
-    arrived = dot(perm[...], drecv[...].reshape(wide, lanes)).astype(BF16)
-    for k in range(kbs):
-        xin[:, lanes * k : lanes * (k + 1)] = arrived[slots * k : slots * (k + 1)]
-    loads[14].wait()
-    loads[15].wait()
     tile = 256
-
-    def up(i, carry):
-        at = pl.ds(pl.multiple_of(i * tile, tile), tile)
-        x = xin[...]
-        gate = jnp.minimum(dot(x, wg[:, at]), LIMIT)
-        lin = jnp.clip(dot(x, wl[:, at]), -LIMIT, LIMIT)
-        hid[:, at] = (gate * jax.nn.sigmoid(ALPHA * gate) * (lin + 1.0)).astype(BF16)
-        return carry
-
-    lax.fori_loop(0, wg.shape[1] // tile, up, 0)
-    loads[16].wait()
-    for k in range(kbs):
-        eo[slots * k : slots * (k + 1)] = dot(
-            hid[...], wd[:, lanes * k : lanes * (k + 1)]
-        ).astype(BF16)
-    rsend[...] = dot(perm_t[...], eo[...]).astype(BF16).reshape(rsend.shape)
-
-    with jax.named_scope("back"):
-        exchange(rsend, rrecv, 4)
+    near = ep // 2
+
+    def expert(at):
+        arrived = dot(perm[...], drecv[at : at + near].reshape(part_rows, lanes)).astype(BF16)
+        for k in range(kbs):
+            xin[:, lanes * k : lanes * (k + 1)] = arrived[slots * k : slots * (k + 1)]
+
+        def up(i, carry):
+            cols = pl.ds(pl.multiple_of(i * tile, tile), tile)
+            x = xin[...]
+            gate = jnp.minimum(dot(x, wg[:, cols]), LIMIT)
+            lin = jnp.clip(dot(x, wl[:, cols]), -LIMIT, LIMIT)
+            hid[:, cols] = (gate * jax.nn.sigmoid(ALPHA * gate) * (lin + 1.0)).astype(BF16)
+            return carry
+
+        lax.fori_loop(0, wg.shape[1] // tile, up, 0)
+        for k in range(kbs):
+            eo[slots * k : slots * (k + 1)] = dot(
+                hid[...], wd[:, lanes * k : lanes * (k + 1)]
+            ).astype(BF16)
+        rsend[at : at + near] = (
+            dot(perm_t[...], eo[...]).astype(BF16).reshape(near, CAP * kbs, lanes)
+        )
+
+    def send_back(j, o):
+        for cc in range(2):
+            copy(rsend.at[2 * j + cc], rrecv.at[me], 5, dev(z - o, cc)).start()
+
+    with jax.named_scope("far_wait"):
+        pltpu.make_async_copy(
+            dsend.at[pl.ds(0, near)], drecv.at[pl.ds(0, near)], recv_sems.at[3]
+        ).wait()
+    for c in loads[14:]:
+        c.wait()
+    with jax.named_scope("far_expert"):
+        expert(0)
+    with jax.named_scope("far_back"):
+        for j in range(near // 2):
+            send_back(j, RING[j])
+    with jax.named_scope("near_wait"):
+        pltpu.make_async_copy(
+            dsend.at[pl.ds(1, near - 1)], drecv.at[pl.ds(1, near - 1)], recv_sems.at[4]
+        ).wait()
+    with jax.named_scope("near_expert"):
+        expert(near)
+    with jax.named_scope("near_back"):
+        for j in range(near // 2, near - 1):
+            send_back(j, RING[j])
+        copy(
+            rsend.at[ep - 1 - core], rrecv.at[me], 5, dev(z, 1 - core)
+        ).start()
+        rrecv[me] = rsend[ep - 2 + core]
     with jax.named_scope("back_wait"):
-        arrive(rsend, rrecv, 4)
+        pltpu.make_async_copy(
+            rsend.at[pl.ds(0, ep - 1)], rrecv.at[pl.ds(0, ep - 1)], recv_sems.at[5]
+        ).wait()
 
     back = rrecv[...].reshape(wide, lanes)
     mixed = dot(combine_hi, back) + dot(combine_lo, back)
@@ -396,13 +397,31 @@
         xbuf.at[pl.ds(0, units)], xbuf.at[pl.ds(0, units)], send_sems.at[0]
     ).wait()
     pltpu.make_async_copy(wbuf.at[pl.ds(0, 5)], wbuf.at[pl.ds(0, 5)], send_sems.at[1]).wait()
+    pltpu.make_async_copy(psend, rbuf, send_sems.at[2]).wait()
     pltpu.make_async_copy(
-        psend.at[pl.ds(0, others)], rbuf.at[pl.ds(0, others)], send_sems.at[2]
+        dsend.at[pl.ds(0, ep // 2)], drecv.at[pl.ds(0, ep // 2)], send_sems.at[3]
     ).wait()
-    for src, dst, phase in ((dsend, drecv, 3), (rsend, rrecv, 4)):
-        pltpu.make_async_copy(
-            src.at[pl.ds(0, ep - 1)], dst.at[pl.ds(0, ep - 1)], send_sems.at[phase]
-        ).wait()
+    pltpu.make_async_copy(
+        dsend.at[pl.ds(1, ep // 2 - 1)], drecv.at[pl.ds(1, ep // 2 - 1)], send_sems.at[4]
+    ).wait()
+    pltpu.make_async_copy(
+        rsend.at[pl.ds(0, ep - 1)], rrecv.at[pl.ds(0, ep - 1)], send_sems.at[5]
+    ).wait()
+
+
+def finish(out_in, state_in, out, state_out, out_buf, state_buf, in_sems, out_sems):
+    rows = state_in.shape[0]
+    ways = [(state_in.at[i], state_buf.at[i], state_out.at[i]) for i in range(rows)]
+    ways.append((out_in, out_buf, out))
+    ins = [pltpu.make_async_copy(w[0], w[1], in_sems.at[i]) for i, w in enumerate(ways)]
+    outs = [pltpu.make_async_copy(w[1], w[2], out_sems.at[i]) for i, w in enumerate(ways)]
+    for c in ins:
+        c.start()
+    for c, d in zip(ins, outs):
+        c.wait()
+        d.start()
+    for d in outs:
+        d.wait()
 
 
 def per_device(
@@ -434,7 +453,7 @@
     vmem = pl.BlockSpec(memory_space=pltpu.VMEM)
     hbm = pl.BlockSpec(memory_space=pltpu.HBM)
     chunks = 2 * len(OFFSETS)
-    return pl.pallas_call(
+    output, new_state = pl.pallas_call(
         functools.partial(kernel, ep),
         out_shape=(
             jax.ShapeDtypeStruct((rows, width), BF16),
@@ -467,14 +486,14 @@
             pltpu.VMEM((ep, CAP * 8, lanes), BF16),
             pltpu.VMEM((ep, CAP * 8, lanes), BF16),
             pltpu.VMEM((ep, CAP * 8, lanes), BF16),
-            pltpu.VMEM((ep * CAP, width), BF16),
-            pltpu.VMEM((ep * CAP, ff), BF16),
-            pltpu.VMEM((wide, lanes), BF16),
-            pltpu.VMEM((wide, wide), BF16),
-            pltpu.VMEM((wide, wide), BF16),
+            pltpu.VMEM((ep // 2 * CAP, width), BF16),
+            pltpu.VMEM((ep // 2 * CAP, ff), BF16),
+            pltpu.VMEM((wide // 2, lanes), BF16),
+            pltpu.VMEM((wide // 2, wide // 2), BF16),
+            pltpu.VMEM((wide // 2, wide // 2), BF16),
             pltpu.SemaphoreType.DMA((17,)),
-            pltpu.SemaphoreType.DMA((5,)),
-            pltpu.SemaphoreType.DMA((5,)),
+            pltpu.SemaphoreType.DMA((6,)),
+            pltpu.SemaphoreType.DMA((6,)),
         ],
         compiler_params=pltpu.CompilerParams(
             collective_id=0, has_side_effects=True, vmem_limit_bytes=63_000_000
@@ -499,6 +518,23 @@
         w_lin_in,
         w_down,
     )
+    return pl.pallas_call(
+        finish,
+        out_shape=(
+            jax.ShapeDtypeStruct((rows, width), BF16),
+            jax.ShapeDtypeStruct(state.shape, F32),
+        ),
+        in_specs=[hbm] * 2,
+        out_specs=(hbm, hbm),
+        scratch_shapes=[
+            pltpu.VMEM((rows, width), BF16),
+            pltpu.VMEM(state.shape, F32),
+            pltpu.SemaphoreType.DMA((rows + 1,)),
+            pltpu.SemaphoreType.DMA((rows + 1,)),
+        ],
+        compiler_params=pltpu.CompilerParams(vmem_limit_bytes=63_000_000),
+        name="finish",
+    )(output, new_state)
 
 
 def solution(mesh):

time: 78.6 us -> 75.4 us (0.959)
  local copies, waits for them, and re-layouts: 4.53 us -> 0 us
  Pallas kernels: 73.2 us -> 74.6 us
    unnamed x2 -> x0, local copies, waits for them, and re-layouts: 4.53 us -> none
    pallas_call x0 -> x1, Pallas kernels: none -> 2.41 us  [per_device(): pl.pallas_call(finish, out_shape=(jax.ShapeDtypeStruct((rows, width), BF1...]
    pallas_call x1, Pallas kernels: 73.2 us -> 72.2 us  [per_device(): pl.pallas_call(functools.partial(kernel, ep), out_shape=(jax.ShapeDtypeSt...]
where the time goes in v3:
time: 75.4 us; the launch traced here: 75.2 us
  Pallas kernels  74.6 us (99%)
    pallas_call x1, Pallas kernels, per_device(): pl.pallas_call(functools.partial(kernel, ep), out_shape=(jax.ShapeDtypeSt...  72.2 us
    pallas_call x1, Pallas kernels, per_device(): pl.pallas_call(finish, out_shape=(jax.ShapeDtypeStruct((rows, width), BF1...  2.41 us

profile of v3, /device:TPU:69, one launch (start us, length us, event | category | flops | bytes accessed | tf_op | source)
XLA Modules:
  0.0 75.2 jit_solution(17198952043544479492)
XLA Ops:
  0.6 72.2 %layer.1 = (bf16[8,2048]{1,0:T(8,128)(2,1)}, f32[8,8,64,128]{3,2,1,0:T(8,128)}) custom-call(bf16[8,2048]{1,0:T(8,128)(2,1)} %tokens_in.1, f32[1,2048]{1,0:T(1,128)} %bitcast.8, bf16[32,2048]{1,0:T(8,128)(2,1)} %bitcast.7, bf16[32,512]{1,0:T(8,128)(2,1)} %w_du_in.1, f32[1,512]{1,0:T(1,128)} %bitcast.10, f32[1,128]{1,0:T(1,128)} %bitcast.13, ...), custom_call_target="tpu_custom_call" | custom-call | tf_op jit(solution)/shard_map/layer/pallas_call | solution.py:456
  72.8 2.4 %finish.1 = (bf16[8,2048]{1,0:T(8,128)(2,1)}, f32[8,8,64,128]{3,2,1,0:T(8,128)}) custom-call(bf16[8,2048]{1,0:T(8,128)(2,1)} %get-tuple-element.4.out_in, f32[8,8,64,128]{3,2,1,0:T(8,128)} %get-tuple-element.5.state_in), custom_call_target="tpu_custom_call" | custom-call | tf_op jit(solution)/shard_map/finish/pallas_call | solution.py:521

commit v4 on v3

--- a/solution.py
+++ b/solution.py
@@ -22,7 +22,6 @@
 
 OFFSETS = (1, 4, 7, -2, -5, -7)
 SEND_ORDER = (2, 5, 4, 1, 3, 0)
-RING = (8, 7, -7, 6, -6, 5, -5, 4, -4, 3, -3, 2, -2, 1, -1, 0)
 
 
 def rms(values, gain):
@@ -83,9 +82,12 @@
     drecv,
     rsend,
     rrecv,
+    st_hi,
+    st_lo,
     xin,
     hid,
-    eo,
+    acc,
+    relay,
     perm,
     perm_t,
     load_sems,
@@ -131,14 +133,13 @@
 
     barrier = pltpu.get_barrier_semaphore()
 
-    def hello(i, carry):
-        pl.semaphore_signal(
-            barrier, inc=1, device_id={"ep": lax.rem(me + i, ep)}, device_id_type=MESH
-        )
-        return carry
+    hops = sorted({abs(o) for o in OFFSETS}, reverse=True)
+    peers = [dev(z + o * g, c) for o in hops for g in (1, -1) for c in range(2)]
+    peers.append(dev(z, 1 - core))
 
     with jax.named_scope("hello"):
-        lax.fori_loop(1, ep, hello, 0)
+        for to in peers:
+            pl.semaphore_signal(barrier, inc=1, device_id=to, device_id_type=MESH)
         for c in loads[5:]:
             c.start()
         for c in loads[:2]:
@@ -154,7 +155,7 @@
         c.wait()
 
     with jax.named_scope("barrier"):
-        pl.semaphore_wait(barrier, ep - 1)
+        pl.semaphore_wait(barrier, len(peers))
 
     def copy(src, dst, phase, device):
         return pltpu.make_async_remote_copy(
@@ -224,11 +225,17 @@
     combine_lo = (combine - combine_hi.astype(F32)).astype(BF16)
     pick = pick.astype(BF16)
 
-    part_rows = wide // 2
-    slots = part_rows // kbs
-    p_r, p_c = iota((part_rows, part_rows), 0), iota((part_rows, part_rows), 1)
+    slots = ep * CAP
+    p_r, p_c = iota((wide, wide), 0), iota((wide, wide), 1)
     perm[...] = (p_c == (lax.rem(p_r, slots) * kbs + p_r // slots)).astype(F32).astype(BF16)
     perm_t[...] = (p_r == (lax.rem(p_c, slots) * kbs + p_c // slots)).astype(F32).astype(BF16)
+
+    loads[12].wait()
+    for h in range(HEADS):
+        s_h = st[:, h].reshape(rows * DK, DV)
+        high = s_h.astype(BF16)
+        st_hi[h] = high
+        st_lo[h] = (s_h - high.astype(F32)).astype(BF16)
 
     chunks = 2 * len(OFFSETS)
     units = 3 * (chunks - 2) + 2
@@ -274,7 +281,6 @@
     keys = sums[0][rows:]
     values = jnp.concatenate([sums[1][:rows], sums[1][rows:]], axis=1)
 
-    loads[12].wait()
     qd = queries * decay
     qk = queries * keys
     block = iota((rows, rows * DK), 1) // DK == iota((rows, rows * DK), 0)
@@ -283,8 +289,10 @@
     for h in range(HEADS):
         q_h = qd[:, DK * h : DK * (h + 1)]
         lhs = jnp.where(block, jnp.concatenate([q_h] * rows, axis=1), 0.0)
-        s_h = st[:, h].reshape(rows * DK, DV)
-        a_h = dot(lhs, s_h, precision=lax.Precision.HIGHEST)
+        lhs_hi = lhs.astype(BF16)
+        lhs_lo = (lhs - lhs_hi.astype(F32)).astype(BF16)
+        both = dot(jnp.concatenate([lhs_hi, lhs_lo], axis=0), st_hi[h])
+        a_h = both[:rows] + both[rows:] + dot(lhs_hi, st_lo[h])
         a_h += jnp.sum(qk[:, DK * h : DK * (h + 1)], axis=1, keepdims=True) * values[
             :, DV * h : DV * (h + 1)
         ]
@@ -295,25 +303,64 @@
     residual = (tok + dot(headed, wo[...])).astype(BF16).astype(F32)
     fed = rms(residual, g_ffn[...])
 
-    lanes = width // kbs
+    lanes = width // (2 * kbs)
+    mid = width // 2
     fed_rows = jnp.concatenate(
-        [fed[:, lanes * k : lanes * (k + 1)] for k in range(kbs)], axis=0
+        [
+            jnp.concatenate(
+                [fed[:, mid * b + lanes * k : mid * b + lanes * (k + 1)] for b in range(2)],
+                axis=1,
+            )
+            for k in range(kbs)
+        ],
+        axis=0,
     ).astype(BF16)
-    dsend[...] = (
-        dot(pick, fed_rows, (((0,), (0,)), ((), ()))).astype(BF16).reshape(dsend.shape)
-    )
+    picked = dot(pick, fed_rows, (((0,), (0,)), ((), ())))
+    for b in range(2):
+        dsend[b] = picked[:, lanes * b : lanes * (b + 1)].astype(BF16).reshape(dsend.shape[1:])
+
+    quarter = chips // 4
+    far_side = range(chips // 2 - 1, quarter, -1)
+    near_side = range(quarter, 0, -1)
+
+    def ring_send(src, dst, phase, o):
+        for cc in range(2):
+            there = wrap(z + o) * 2 + cc
+            copy(src.at[there], dst.at[me], phase, {"ep": there}).start()
+
+    def send_up(src, dst, phase):
+        there = wrap(z + chips // 2) * 2
+        copy(src.at[there], dst.at[me], phase, {"ep": there}).start()
+        for o in range(chips // 2 - 1, 0, -1):
+            ring_send(src, dst, phase, o)
+        there = 2 * z + 1 - core
+        copy(src.at[there], dst.at[me], phase, {"ep": there}).start()
+        dst[me] = src[me]
+
+    def send_relay(src, via, phase):
+        there = wrap(z + chips // 2) * 2 + 1
+        copy(src.at[there], via, phase, dev(z - quarter, core)).start()
+
+    def send_down(src, dst, phase, side):
+        for o in side:
+            ring_send(src, dst, phase, -o)
+
+    def forward(via, relay_phase, dst, phase):
+        pltpu.make_async_copy(via, via, recv_sems.at[relay_phase]).wait()
+        origin = wrap(z + quarter) * 2 + core
+        copy(via, dst.at[origin], phase, dev(z - quarter, 1)).start()
+
+    def arrive(src, dst, phase):
+        pltpu.make_async_copy(
+            src.at[pl.ds(0, ep - 1)], dst.at[pl.ds(0, ep - 1)], recv_sems.at[phase]
+        ).wait()
 
     with jax.named_scope("dispatch"):
-        for j, o in enumerate(RING):
-            for cc in range(2):
-                there = wrap(z + o) * 2 + cc
-                if o:
-                    copy(
-                        dsend.at[there], drecv.at[2 * j + core], 3 + j // (ep // 4), {"ep": there}
-                    ).start()
-        there = 2 * z + 1 - core
-        copy(dsend.at[there], drecv.at[ep - 2 + core], 4, {"ep": there}).start()
-        drecv[ep - 2 + core] = dsend[me]
+        for b in range(2):
+            send_relay(dsend.at[b], relay.at[b], 7 + b)
+            send_up(dsend.at[b], drecv.at[b], 3 + b)
+            if b == 0:
+                send_down(dsend.at[b], drecv.at[b], 3 + b, far_side)
 
     with jax.named_scope("new_state"):
         decay_cols, key_cols = decay.T, keys.T
@@ -324,73 +371,84 @@
                     decay_cols[at, t : t + 1] * st[t, h]
                     + key_cols[at, t : t + 1] * values[t : t + 1, DV * h : DV * (h + 1)]
                 )
-
         store = pltpu.make_async_copy(st, state_out, load_sems.at[12])
         store.start()
 
+    with jax.named_scope("dispatch_relay"):
+        forward(relay.at[0], 7, drecv.at[0], 3)
+        send_down(dsend.at[0], drecv.at[0], 3, near_side)
+        send_down(dsend.at[1], drecv.at[1], 4, far_side)
+        forward(relay.at[1], 8, drecv.at[1], 4)
+        send_down(dsend.at[1], drecv.at[1], 4, near_side)
+
     tile = 256
-    near = ep // 2
-
-    def expert(at):
-        arrived = dot(perm[...], drecv[at : at + near].reshape(part_rows, lanes)).astype(BF16)
+
+    def up(b):
+        half_in = slice(mid * b, mid * (b + 1))
+        arrived = dot(perm[...], drecv[b].reshape(wide, lanes)).astype(BF16)
         for k in range(kbs):
-            xin[:, lanes * k : lanes * (k + 1)] = arrived[slots * k : slots * (k + 1)]
-
-        def up(i, carry):
+            xin[:, mid * b + lanes * k : mid * b + lanes * (k + 1)] = arrived[
+                slots * k : slots * (k + 1)
+            ]
+
+        def step(i, carry):
             cols = pl.ds(pl.multiple_of(i * tile, tile), tile)
-            x = xin[...]
-            gate = jnp.minimum(dot(x, wg[:, cols]), LIMIT)
-            lin = jnp.clip(dot(x, wl[:, cols]), -LIMIT, LIMIT)
-            hid[:, cols] = (gate * jax.nn.sigmoid(ALPHA * gate) * (lin + 1.0)).astype(BF16)
+            x = xin[:, half_in]
+            gate, lin = dot(x, wg[half_in, cols]), dot(x, wl[half_in, cols])
+            if b == 0:
+                acc[0, :, cols] = gate
+                acc[1, :, cols] = lin
+            else:
+                gate = jnp.minimum(gate + acc[0, :, cols], LIMIT)
+                lin = jnp.clip(lin + acc[1, :, cols], -LIMIT, LIMIT)
+                hid[:, cols] = (gate * jax.nn.sigmoid(ALPHA * gate) * (lin + 1.0)).astype(BF16)
             return carry
 
-        lax.fori_loop(0, wg.shape[1] // tile, up, 0)
-        for k in range(kbs):
-            eo[slots * k : slots * (k + 1)] = dot(
-                hid[...], wd[:, lanes * k : lanes * (k + 1)]
-            ).astype(BF16)
-        rsend[at : at + near] = (
-            dot(perm_t[...], eo[...]).astype(BF16).reshape(near, CAP * kbs, lanes)
-        )
-
-    def send_back(j, o):
-        for cc in range(2):
-            copy(rsend.at[2 * j + cc], rrecv.at[me], 5, dev(z - o, cc)).start()
-
-    with jax.named_scope("far_wait"):
-        pltpu.make_async_copy(
-            dsend.at[pl.ds(0, near)], drecv.at[pl.ds(0, near)], recv_sems.at[3]
-        ).wait()
+        lax.fori_loop(0, wg.shape[1] // tile, step, 0)
+
+    def down(b):
+        blocks = []
+        for at in range(mid * b, mid * (b + 1), tile):
+            both = dot(hid[...], wd[:, at : at + tile])
+            blocks += [both[:, lanes * k : lanes * (k + 1)] for k in range(tile // lanes)]
+        expert_out = jnp.concatenate(blocks, axis=0).astype(BF16)
+        rsend[b] = dot(perm_t[...], expert_out).astype(BF16).reshape(rsend.shape[1:])
+
+    with jax.named_scope("half_wait"):
+        arrive(dsend.at[0], drecv.at[0], 3)
     for c in loads[14:]:
         c.wait()
-    with jax.named_scope("far_expert"):
-        expert(0)
-    with jax.named_scope("far_back"):
-        for j in range(near // 2):
-            send_back(j, RING[j])
-    with jax.named_scope("near_wait"):
-        pltpu.make_async_copy(
-            dsend.at[pl.ds(1, near - 1)], drecv.at[pl.ds(1, near - 1)], recv_sems.at[4]
-        ).wait()
-    with jax.named_scope("near_expert"):
-        expert(near)
-    with jax.named_scope("near_back"):
-        for j in range(near // 2, near - 1):
-            send_back(j, RING[j])
-        copy(
-            rsend.at[ep - 1 - core], rrecv.at[me], 5, dev(z, 1 - core)
-        ).start()
-        rrecv[me] = rsend[ep - 2 + core]
-    with jax.named_scope("back_wait"):
-        pltpu.make_async_copy(
-            rsend.at[pl.ds(0, ep - 1)], rrecv.at[pl.ds(0, ep - 1)], recv_sems.at[5]
-        ).wait()
-
-    back = rrecv[...].reshape(wide, lanes)
-    mixed = dot(combine_hi, back) + dot(combine_lo, back)
-    for k in range(kbs):
-        at = slice(lanes * k, lanes * (k + 1))
-        out[:, at] = (residual[:, at] + mixed[rows * k : rows * (k + 1)]).astype(BF16)
+    with jax.named_scope("half_up"):
+        up(0)
+    with jax.named_scope("full_wait"):
+        arrive(dsend.at[1], drecv.at[1], 4)
+    with jax.named_scope("full_up"):
+        up(1)
+    with jax.named_scope("down"):
+        down(0)
+    with jax.named_scope("half_back"):
+        send_relay(rsend.at[0], relay.at[2], 9)
+        send_up(rsend.at[0], rrecv.at[0], 5)
+        send_down(rsend.at[0], rrecv.at[0], 5, far_side)
+    with jax.named_scope("down_rest"):
+        down(1)
+    with jax.named_scope("full_back"):
+        send_relay(rsend.at[1], relay.at[3], 10)
+        send_up(rsend.at[1], rrecv.at[1], 6)
+        forward(relay.at[2], 9, rrecv.at[0], 5)
+        send_down(rsend.at[0], rrecv.at[0], 5, near_side)
+        send_down(rsend.at[1], rrecv.at[1], 6, far_side)
+        forward(relay.at[3], 10, rrecv.at[1], 6)
+        send_down(rsend.at[1], rrecv.at[1], 6, near_side)
+
+    for b in range(2):
+        with jax.named_scope("back_wait"):
+            arrive(rsend.at[b], rrecv.at[b], 5 + b)
+        back = rrecv[b].reshape(wide, lanes)
+        mixed = dot(combine_hi, back) + dot(combine_lo, back)
+        for k in range(kbs):
+            at = slice(mid * b + lanes * k, mid * b + lanes * (k + 1))
+            out[:, at] = (residual[:, at] + mixed[rows * k : rows * (k + 1)]).astype(BF16)
 
     store.wait()
     pltpu.make_async_copy(
@@ -398,15 +456,13 @@
     ).wait()
     pltpu.make_async_copy(wbuf.at[pl.ds(0, 5)], wbuf.at[pl.ds(0, 5)], send_sems.at[1]).wait()
     pltpu.make_async_copy(psend, rbuf, send_sems.at[2]).wait()
-    pltpu.make_async_copy(
-        dsend.at[pl.ds(0, ep // 2)], drecv.at[pl.ds(0, ep // 2)], send_sems.at[3]
-    ).wait()
-    pltpu.make_async_copy(
-        dsend.at[pl.ds(1, ep // 2 - 1)], drecv.at[pl.ds(1, ep // 2 - 1)], send_sems.at[4]
-    ).wait()
-    pltpu.make_async_copy(
-        rsend.at[pl.ds(0, ep - 1)], rrecv.at[pl.ds(0, ep - 1)], send_sems.at[5]
-    ).wait()
+    for b in range(2):
+        for src, dst, phase in ((dsend, drecv, 3), (rsend, rrecv, 5)):
+            pltpu.make_async_copy(
+                src.at[b, pl.ds(0, ep - 1)], dst.at[b, pl.ds(0, ep - 1)], send_sems.at[phase + b]
+            ).wait()
+        for i in (b, 2 + b):
+            pltpu.make_async_copy(relay.at[i], relay.at[i], send_sems.at[7 + i]).wait()
 
 
 def finish(out_in, state_in, out, state_out, out_buf, state_buf, in_sems, out_sems):
@@ -448,7 +504,7 @@
     share, qk = w_query.shape
     vw = w_value.shape[1]
     ff = w_gate_in.shape[2]
-    lanes = width // 8
+    lanes = width // 16
     wide = ep * CAP * 8
     vmem = pl.BlockSpec(memory_space=pltpu.VMEM)
     hbm = pl.BlockSpec(memory_space=pltpu.HBM)
@@ -482,18 +538,21 @@
             pltpu.VMEM((6, share, vw), BF16),
             pltpu.VMEM((chunks, 2 * rows, vw // 2), BF16),
             pltpu.VMEM((chunks, 2 * rows, vw // 2), BF16),
-            pltpu.VMEM((ep, CAP * 8, lanes), BF16),
-            pltpu.VMEM((ep, CAP * 8, lanes), BF16),
-            pltpu.VMEM((ep, CAP * 8, lanes), BF16),
-            pltpu.VMEM((ep, CAP * 8, lanes), BF16),
-            pltpu.VMEM((ep // 2 * CAP, width), BF16),
-            pltpu.VMEM((ep // 2 * CAP, ff), BF16),
-            pltpu.VMEM((wide // 2, lanes), BF16),
-            pltpu.VMEM((wide // 2, wide // 2), BF16),
-            pltpu.VMEM((wide // 2, wide // 2), BF16),
+            pltpu.VMEM((2, ep, CAP * 8, lanes), BF16),
+            pltpu.VMEM((2, ep, CAP * 8, lanes), BF16),
+            pltpu.VMEM((2, ep, CAP * 8, lanes), BF16),
+            pltpu.VMEM((2, ep, CAP * 8, lanes), BF16),
+            pltpu.VMEM((HEADS, rows * DK, DV), BF16),
+            pltpu.VMEM((HEADS, rows * DK, DV), BF16),
+            pltpu.VMEM((ep * CAP, width), BF16),
+            pltpu.VMEM((ep * CAP, ff), BF16),
+            pltpu.VMEM((2, ep * CAP, ff), F32),
+            pltpu.VMEM((4, CAP * 8, lanes), BF16),
+            pltpu.VMEM((wide, wide), BF16),
+            pltpu.VMEM((wide, wide), BF16),
             pltpu.SemaphoreType.DMA((17,)),
-            pltpu.SemaphoreType.DMA((6,)),
-            pltpu.SemaphoreType.DMA((6,)),
+            pltpu.SemaphoreType.DMA((11,)),
+            pltpu.SemaphoreType.DMA((11,)),
         ],
         compiler_params=pltpu.CompilerParams(
             collective_id=0, has_side_effects=True, vmem_limit_bytes=63_000_000

time: 75.4 us -> 76.7 us (1.017)
  Pallas kernels: 74.6 us -> 75.9 us
    pallas_call x1, Pallas kernels: 72.2 us -> 73.5 us  [per_device(): pl.pallas_call(functools.partial(kernel, ep), out_shape=(jax.ShapeDtypeSt...]
where the time goes in v4:
time: 76.7 us; the launch traced here: 76.5 us
  Pallas kernels  75.9 us (99%)
    pallas_call x1, Pallas kernels, per_device(): pl.pallas_call(functools.partial(kernel, ep), out_shape=(jax.ShapeDtypeSt...  73.5 us
    pallas_call x1, Pallas kernels, per_device(): pl.pallas_call(finish, out_shape=(jax.ShapeDtypeStruct((rows, width), BF1...  2.41 us

profile of v4, /device:TPU:69, one launch (start us, length us, event | category | flops | bytes accessed | tf_op | source)
XLA Modules:
  0.0 76.5 jit_solution(16467743857659688200)
XLA Ops:
  0.6 73.5 %layer.1 = (bf16[8,2048]{1,0:T(8,128)(2,1)}, f32[8,8,64,128]{3,2,1,0:T(8,128)}) custom-call(bf16[8,2048]{1,0:T(8,128)(2,1)} %tokens_in.1, f32[1,2048]{1,0:T(1,128)} %bitcast.8, bf16[32,2048]{1,0:T(8,128)(2,1)} %bitcast.7, bf16[32,512]{1,0:T(8,128)(2,1)} %w_du_in.1, f32[1,512]{1,0:T(1,128)} %bitcast.10, f32[1,128]{1,0:T(1,128)} %bitcast.13, ...), custom_call_target="tpu_custom_call" | custom-call | tf_op jit(solution)/shard_map/layer/pallas_call | solution.py:512
  74.1 2.4 %finish.1 = (bf16[8,2048]{1,0:T(8,128)(2,1)}, f32[8,8,64,128]{3,2,1,0:T(8,128)}) custom-call(bf16[8,2048]{1,0:T(8,128)(2,1)} %get-tuple-element.4.out_in, f32[8,8,64,128]{3,2,1,0:T(8,128)} %get-tuple-element.5.state_in), custom_call_target="tpu_custom_call" | custom-call | tf_op jit(solution)/shard_map/finish/pallas_call | solution.py:580

commit v5 on v3

--- a/solution.py
+++ b/solution.py
@@ -22,7 +22,6 @@
 
 OFFSETS = (1, 4, 7, -2, -5, -7)
 SEND_ORDER = (2, 5, 4, 1, 3, 0)
-RING = (8, 7, -7, 6, -6, 5, -5, 4, -4, 3, -3, 2, -2, 1, -1, 0)
 
 
 def rms(values, gain):
@@ -83,9 +82,10 @@
     drecv,
     rsend,
     rrecv,
+    st_hi,
+    st_lo,
     xin,
     hid,
-    eo,
     perm,
     perm_t,
     load_sems,
@@ -131,14 +131,13 @@
 
     barrier = pltpu.get_barrier_semaphore()
 
-    def hello(i, carry):
-        pl.semaphore_signal(
-            barrier, inc=1, device_id={"ep": lax.rem(me + i, ep)}, device_id_type=MESH
-        )
-        return carry
+    hops = sorted({abs(o) for o in OFFSETS}, reverse=True)
+    peers = [dev(z + o * g, c) for o in hops for g in (1, -1) for c in range(2)]
+    peers.append(dev(z, 1 - core))
 
     with jax.named_scope("hello"):
-        lax.fori_loop(1, ep, hello, 0)
+        for to in peers:
+            pl.semaphore_signal(barrier, inc=1, device_id=to, device_id_type=MESH)
         for c in loads[5:]:
             c.start()
         for c in loads[:2]:
@@ -154,7 +153,7 @@
         c.wait()
 
     with jax.named_scope("barrier"):
-        pl.semaphore_wait(barrier, ep - 1)
+        pl.semaphore_wait(barrier, len(peers))
 
     def copy(src, dst, phase, device):
         return pltpu.make_async_remote_copy(
@@ -166,8 +165,8 @@
             device_id_type=MESH,
         )
 
-    for oi in SEND_ORDER:
-        for cc in range(2):
+    for cc in range(2):
+        for oi in SEND_ORDER:
             zz = wrap(z + (1 - 2 * cc) * OFFSETS[oi])
             slot = 3 * (2 * oi + core)
             if oi == len(OFFSETS) - 1:
@@ -175,8 +174,7 @@
             else:
                 src, dst = xs.at[pl.ds(zz, 3)], xbuf.at[pl.ds(slot, 3)]
             copy(src, dst, 0, dev(zz, cc)).start()
-    for n in (1, -1):
-        for cc in range(2):
+        for n in (1, -1):
             copy(own_w.at[cc], wbuf.at[2 * (1 - n) + core], 1, dev(z + n, cc)).start()
     copy(own_w.at[1 - core], wbuf.at[2 + core], 1, dev(z, 1 - core)).start()
 
@@ -224,11 +222,17 @@
     combine_lo = (combine - combine_hi.astype(F32)).astype(BF16)
     pick = pick.astype(BF16)
 
-    part_rows = wide // 2
-    slots = part_rows // kbs
-    p_r, p_c = iota((part_rows, part_rows), 0), iota((part_rows, part_rows), 1)
+    slots = ep * CAP
+    p_r, p_c = iota((wide, wide), 0), iota((wide, wide), 1)
     perm[...] = (p_c == (lax.rem(p_r, slots) * kbs + p_r // slots)).astype(F32).astype(BF16)
     perm_t[...] = (p_r == (lax.rem(p_c, slots) * kbs + p_c // slots)).astype(F32).astype(BF16)
+
+    loads[12].wait()
+    for h in range(HEADS):
+        s_h = st[:, h].reshape(rows * DK, DV)
+        high = s_h.astype(BF16)
+        st_hi[h] = high
+        st_lo[h] = (s_h - high.astype(F32)).astype(BF16)
 
     chunks = 2 * len(OFFSETS)
     units = 3 * (chunks - 2) + 2
@@ -255,8 +259,8 @@
             [one[:, : cols // 2], one[:, cols // 2 :]], axis=0
         ).astype(BF16)
     sign = 1 - 2 * core
-    for oi in SEND_ORDER:
-        for cc in range(2):
+    for cc in range(2):
+        for oi in SEND_ORDER:
             to = dev(z - sign * OFFSETS[oi], cc)
             copy(psend.at[2 * oi + cc], rbuf.at[2 * oi + core], 2, to).start()
     with jax.named_scope("partials_wait"):
@@ -274,7 +278,6 @@
     keys = sums[0][rows:]
     values = jnp.concatenate([sums[1][:rows], sums[1][rows:]], axis=1)
 
-    loads[12].wait()
     qd = queries * decay
     qk = queries * keys
     block = iota((rows, rows * DK), 1) // DK == iota((rows, rows * DK), 0)
@@ -283,8 +286,10 @@
     for h in range(HEADS):
         q_h = qd[:, DK * h : DK * (h + 1)]
         lhs = jnp.where(block, jnp.concatenate([q_h] * rows, axis=1), 0.0)
-        s_h = st[:, h].reshape(rows * DK, DV)
-        a_h = dot(lhs, s_h, precision=lax.Precision.HIGHEST)
+        lhs_hi = lhs.astype(BF16)
+        lhs_lo = (lhs - lhs_hi.astype(F32)).astype(BF16)
+        both = dot(jnp.concatenate([lhs_hi, lhs_lo], axis=0), st_hi[h])
+        a_h = both[:rows] + both[rows:] + dot(lhs_hi, st_lo[h])
         a_h += jnp.sum(qk[:, DK * h : DK * (h + 1)], axis=1, keepdims=True) * values[
             :, DV * h : DV * (h + 1)
         ]
@@ -303,17 +308,23 @@
         dot(pick, fed_rows, (((0,), (0,)), ((), ()))).astype(BF16).reshape(dsend.shape)
     )
 
+    def exchange(src, dst, phase):
+        for cc in range(2):
+            for o in range(chips // 2, 0, -1):
+                for oo in (o, -o)[: 1 + (o < chips // 2)]:
+                    there = wrap(z + oo) * 2 + cc
+                    copy(src.at[there], dst.at[me], phase, {"ep": there}).start()
+        there = 2 * z + 1 - core
+        copy(src.at[there], dst.at[me], phase, {"ep": there}).start()
+        dst[me] = src[me]
+
+    def arrive(src, dst, phase):
+        pltpu.make_async_copy(
+            src.at[pl.ds(0, ep - 1)], dst.at[pl.ds(0, ep - 1)], recv_sems.at[phase]
+        ).wait()
+
     with jax.named_scope("dispatch"):
-        for j, o in enumerate(RING):
-            for cc in range(2):
-                there = wrap(z + o) * 2 + cc
-                if o:
-                    copy(
-                        dsend.at[there], drecv.at[2 * j + core], 3 + j // (ep // 4), {"ep": there}
-                    ).start()
-        there = 2 * z + 1 - core
-        copy(dsend.at[there], drecv.at[ep - 2 + core], 4, {"ep": there}).start()
-        drecv[ep - 2 + core] = dsend[me]
+        exchange(dsend, drecv, 3)
 
     with jax.named_scope("new_state"):
         decay_cols, key_cols = decay.T, keys.T
@@ -324,17 +335,18 @@
                     decay_cols[at, t : t + 1] * st[t, h]
                     + key_cols[at, t : t + 1] * values[t : t + 1, DV * h : DV * (h + 1)]
                 )
-
         store = pltpu.make_async_copy(st, state_out, load_sems.at[12])
         store.start()
 
-    tile = 256
-    near = ep // 2
-
-    def expert(at):
-        arrived = dot(perm[...], drecv[at : at + near].reshape(part_rows, lanes)).astype(BF16)
+    with jax.named_scope("dispatch_wait"):
+        arrive(dsend, drecv, 3)
+    with jax.named_scope("expert"):
+        arrived = dot(perm[...], drecv[...].reshape(wide, lanes)).astype(BF16)
         for k in range(kbs):
             xin[:, lanes * k : lanes * (k + 1)] = arrived[slots * k : slots * (k + 1)]
+        for c in loads[14:]:
+            c.wait()
+        tile = 256
 
         def up(i, carry):
             cols = pl.ds(pl.multiple_of(i * tile, tile), tile)
@@ -345,46 +357,14 @@
             return carry
 
         lax.fori_loop(0, wg.shape[1] // tile, up, 0)
-        for k in range(kbs):
-            eo[slots * k : slots * (k + 1)] = dot(
-                hid[...], wd[:, lanes * k : lanes * (k + 1)]
-            ).astype(BF16)
-        rsend[at : at + near] = (
-            dot(perm_t[...], eo[...]).astype(BF16).reshape(near, CAP * kbs, lanes)
-        )
-
-    def send_back(j, o):
-        for cc in range(2):
-            copy(rsend.at[2 * j + cc], rrecv.at[me], 5, dev(z - o, cc)).start()
-
-    with jax.named_scope("far_wait"):
-        pltpu.make_async_copy(
-            dsend.at[pl.ds(0, near)], drecv.at[pl.ds(0, near)], recv_sems.at[3]
-        ).wait()
-    for c in loads[14:]:
-        c.wait()
-    with jax.named_scope("far_expert"):
-        expert(0)
-    with jax.named_scope("far_back"):
-        for j in range(near // 2):
-            send_back(j, RING[j])
-    with jax.named_scope("near_wait"):
-        pltpu.make_async_copy(
-            dsend.at[pl.ds(1, near - 1)], drecv.at[pl.ds(1, near - 1)], recv_sems.at[4]
-        ).wait()
-    with jax.named_scope("near_expert"):
-        expert(near)
-    with jax.named_scope("near_back"):
-        for j in range(near // 2, near - 1):
-            send_back(j, RING[j])
-        copy(
-            rsend.at[ep - 1 - core], rrecv.at[me], 5, dev(z, 1 - core)
-        ).start()
-        rrecv[me] = rsend[ep - 2 + core]
+        expert_out = jnp.concatenate(
+            [dot(hid[...], wd[:, lanes * k : lanes * (k + 1)]) for k in range(kbs)], axis=0
+        ).astype(BF16)
+        rsend[...] = dot(perm_t[...], expert_out).astype(BF16).reshape(rsend.shape)
+    with jax.named_scope("back"):
+        exchange(rsend, rrecv, 4)
     with jax.named_scope("back_wait"):
-        pltpu.make_async_copy(
-            rsend.at[pl.ds(0, ep - 1)], rrecv.at[pl.ds(0, ep - 1)], recv_sems.at[5]
-        ).wait()
+        arrive(rsend, rrecv, 4)
 
     back = rrecv[...].reshape(wide, lanes)
     mixed = dot(combine_hi, back) + dot(combine_lo, back)
@@ -398,15 +378,10 @@
     ).wait()
     pltpu.make_async_copy(wbuf.at[pl.ds(0, 5)], wbuf.at[pl.ds(0, 5)], send_sems.at[1]).wait()
     pltpu.make_async_copy(psend, rbuf, send_sems.at[2]).wait()
-    pltpu.make_async_copy(
-        dsend.at[pl.ds(0, ep // 2)], drecv.at[pl.ds(0, ep // 2)], send_sems.at[3]
-    ).wait()
-    pltpu.make_async_copy(
-        dsend.at[pl.ds(1, ep // 2 - 1)], drecv.at[pl.ds(1, ep // 2 - 1)], send_sems.at[4]
-    ).wait()
-    pltpu.make_async_copy(
-        rsend.at[pl.ds(0, ep - 1)], rrecv.at[pl.ds(0, ep - 1)], send_sems.at[5]
-    ).wait()
+    for src, dst, phase in ((dsend, drecv, 3), (rsend, rrecv, 4)):
+        pltpu.make_async_copy(
+            src.at[pl.ds(0, ep - 1)], dst.at[pl.ds(0, ep - 1)], send_sems.at[phase]
+        ).wait()
 
 
 def finish(out_in, state_in, out, state_out, out_buf, state_buf, in_sems, out_sems):
@@ -486,14 +461,15 @@
             pltpu.VMEM((ep, CAP * 8, lanes), BF16),
             pltpu.VMEM((ep, CAP * 8, lanes), BF16),
             pltpu.VMEM((ep, CAP * 8, lanes), BF16),
-            pltpu.VMEM((ep // 2 * CAP, width), BF16),
-            pltpu.VMEM((ep // 2 * CAP, ff), BF16),
-            pltpu.VMEM((wide // 2, lanes), BF16),
-            pltpu.VMEM((wide // 2, wide // 2), BF16),
-            pltpu.VMEM((wide // 2, wide // 2), BF16),
+            pltpu.VMEM((HEADS, rows * DK, DV), BF16),
+            pltpu.VMEM((HEADS, rows * DK, DV), BF16),
+            pltpu.VMEM((ep * CAP, width), BF16),
+            pltpu.VMEM((ep * CAP, ff), BF16),
+            pltpu.VMEM((wide, wide), BF16),
+            pltpu.VMEM((wide, wide), BF16),
             pltpu.SemaphoreType.DMA((17,)),
-            pltpu.SemaphoreType.DMA((6,)),
-            pltpu.SemaphoreType.DMA((6,)),
+            pltpu.SemaphoreType.DMA((5,)),
+            pltpu.SemaphoreType.DMA((5,)),
         ],
         compiler_params=pltpu.CompilerParams(
             collective_id=0, has_side_effects=True, vmem_limit_bytes=63_000_000

time: 75.4 us -> 72 us (0.955)
  Pallas kernels: 74.6 us -> 71.2 us
    pallas_call x1, Pallas kernels: 72.2 us -> 68.8 us  [per_device(): pl.pallas_call(functools.partial(kernel, ep), out_shape=(jax.ShapeDtypeSt...]
where the time goes in v5:
time: 72 us; the launch traced here: 71.9 us
  Pallas kernels  71.2 us (99%)
    pallas_call x1, Pallas kernels, per_device(): pl.pallas_call(functools.partial(kernel, ep), out_shape=(jax.ShapeDtypeSt...  68.8 us
    pallas_call x1, Pallas kernels, per_device(): pl.pallas_call(finish, out_shape=(jax.ShapeDtypeStruct((rows, width), BF1...  2.41 us

profile of v5, /device:TPU:69, one launch (start us, length us, event | category | flops | bytes accessed | tf_op | source)
XLA Modules:
  0.0 71.9 jit_solution(17170414019264270191)
XLA Ops:
  0.6 68.8 %layer.1 = (bf16[8,2048]{1,0:T(8,128)(2,1)}, f32[8,8,64,128]{3,2,1,0:T(8,128)}) custom-call(bf16[8,2048]{1,0:T(8,128)(2,1)} %tokens_in.1, f32[1,2048]{1,0:T(1,128)} %bitcast.8, bf16[32,2048]{1,0:T(8,128)(2,1)} %bitcast.7, bf16[32,512]{1,0:T(8,128)(2,1)} %w_du_in.1, f32[1,512]{1,0:T(1,128)} %bitcast.10, f32[1,128]{1,0:T(1,128)} %bitcast.13, ...), custom_call_target="tpu_custom_call" | custom-call | tf_op jit(solution)/shard_map/layer/pallas_call | solution.py:431
  69.5 2.4 %finish.1 = (bf16[8,2048]{1,0:T(8,128)(2,1)}, f32[8,8,64,128]{3,2,1,0:T(8,128)}) custom-call(bf16[8,2048]{1,0:T(8,128)(2,1)} %get-tuple-element.4.out_in, f32[8,8,64,128]{3,2,1,0:T(8,128)} %get-tuple-element.5.state_in), custom_call_target="tpu_custom_call" | custom-call | tf_op jit(solution)/shard_map/finish/pallas_call | solution.py:497

commit v6 on v5

--- a/solution.py
+++ b/solution.py
@@ -126,9 +126,6 @@
     loads = [
         pltpu.make_async_copy(src, dst, load_sems.at[i]) for i, (src, dst) in enumerate(pairs)
     ]
-    for c in loads[:5]:
-        c.start()
-
     barrier = pltpu.get_barrier_semaphore()
 
     hops = sorted({abs(o) for o in OFFSETS}, reverse=True)
@@ -138,7 +135,7 @@
     with jax.named_scope("hello"):
         for to in peers:
             pl.semaphore_signal(barrier, inc=1, device_id=to, device_id_type=MESH)
-        for c in loads[5:]:
+        for c in loads:
             c.start()
         for c in loads[:2]:
             c.wait()
@@ -165,8 +162,8 @@
             device_id_type=MESH,
         )
 
-    for cc in range(2):
-        for oi in SEND_ORDER:
+    for oi in SEND_ORDER:
+        for cc in range(2):
             zz = wrap(z + (1 - 2 * cc) * OFFSETS[oi])
             slot = 3 * (2 * oi + core)
             if oi == len(OFFSETS) - 1:
@@ -174,7 +171,8 @@
             else:
                 src, dst = xs.at[pl.ds(zz, 3)], xbuf.at[pl.ds(slot, 3)]
             copy(src, dst, 0, dev(zz, cc)).start()
-        for n in (1, -1):
+    for n in (1, -1):
+        for cc in range(2):
             copy(own_w.at[cc], wbuf.at[2 * (1 - n) + core], 1, dev(z + n, cc)).start()
     copy(own_w.at[1 - core], wbuf.at[2 + core], 1, dev(z, 1 - core)).start()
 
@@ -222,8 +220,9 @@
     combine_lo = (combine - combine_hi.astype(F32)).astype(BF16)
     pick = pick.astype(BF16)
 
-    slots = ep * CAP
-    p_r, p_c = iota((wide, wide), 0), iota((wide, wide), 1)
+    group = wide // 2
+    slots = group // kbs
+    p_r, p_c = iota((group, group), 0), iota((group, group), 1)
     perm[...] = (p_c == (lax.rem(p_r, slots) * kbs + p_r // slots)).astype(F32).astype(BF16)
     perm_t[...] = (p_r == (lax.rem(p_c, slots) * kbs + p_c // slots)).astype(F32).astype(BF16)
 
@@ -308,12 +307,13 @@
         dot(pick, fed_rows, (((0,), (0,)), ((), ()))).astype(BF16).reshape(dsend.shape)
     )
 
-    def exchange(src, dst, phase):
-        for cc in range(2):
-            for o in range(chips // 2, 0, -1):
-                for oo in (o, -o)[: 1 + (o < chips // 2)]:
-                    there = wrap(z + oo) * 2 + cc
-                    copy(src.at[there], dst.at[me], phase, {"ep": there}).start()
+    ring = [o * g for o in range(chips // 2, 0, -1) for g in (1, -1)]
+    ring.remove(-(chips // 2))
+
+    def exchange(src, dst, phase, targets):
+        for o, cc in targets:
+            there = wrap(z + o) * 2 + cc
+            copy(src.at[there], dst.at[me], phase, {"ep": there}).start()
         there = 2 * z + 1 - core
         copy(src.at[there], dst.at[me], phase, {"ep": there}).start()
         dst[me] = src[me]
@@ -324,7 +324,7 @@
         ).wait()
 
     with jax.named_scope("dispatch"):
-        exchange(dsend, drecv, 3)
+        exchange(dsend, drecv, 3, [(o, cc) for cc in range(2) for o in ring])
 
     with jax.named_scope("new_state"):
         decay_cols, key_cols = decay.T, keys.T
@@ -341,28 +341,33 @@
     with jax.named_scope("dispatch_wait"):
         arrive(dsend, drecv, 3)
     with jax.named_scope("expert"):
-        arrived = dot(perm[...], drecv[...].reshape(wide, lanes)).astype(BF16)
-        for k in range(kbs):
-            xin[:, lanes * k : lanes * (k + 1)] = arrived[slots * k : slots * (k + 1)]
+        some = ep // 2
+        for g in range(2):
+            came = drecv[some * g : some * (g + 1)].reshape(group, lanes)
+            arrived = dot(perm[...], came).astype(BF16)
+            for k in range(kbs):
+                xin[slots * g : slots * (g + 1), lanes * k : lanes * (k + 1)] = arrived[
+                    slots * k : slots * (k + 1)
+                ]
         for c in loads[14:]:
             c.wait()
         tile = 256
-
-        def up(i, carry):
-            cols = pl.ds(pl.multiple_of(i * tile, tile), tile)
+        for at in range(0, wg.shape[1], tile):
+            cols = slice(at, at + tile)
             x = xin[...]
             gate = jnp.minimum(dot(x, wg[:, cols]), LIMIT)
             lin = jnp.clip(dot(x, wl[:, cols]), -LIMIT, LIMIT)
             hid[:, cols] = (gate * jax.nn.sigmoid(ALPHA * gate) * (lin + 1.0)).astype(BF16)
-            return carry
-
-        lax.fori_loop(0, wg.shape[1] // tile, up, 0)
-        expert_out = jnp.concatenate(
-            [dot(hid[...], wd[:, lanes * k : lanes * (k + 1)]) for k in range(kbs)], axis=0
-        ).astype(BF16)
-        rsend[...] = dot(perm_t[...], expert_out).astype(BF16).reshape(rsend.shape)
+        made = [dot(hid[...], wd[:, lanes * k : lanes * (k + 1)]) for k in range(kbs)]
+        for g in range(2):
+            expert_out = jnp.concatenate(
+                [m[slots * g : slots * (g + 1)] for m in made], axis=0
+            ).astype(BF16)
+            rsend[some * g : some * (g + 1)] = (
+                dot(perm_t[...], expert_out).astype(BF16).reshape(some, CAP * kbs, lanes)
+            )
     with jax.named_scope("back"):
-        exchange(rsend, rrecv, 4)
+        exchange(rsend, rrecv, 4, [(o, cc) for o in ring for cc in range(2)])
     with jax.named_scope("back_wait"):
         arrive(rsend, rrecv, 4)
 
@@ -465,8 +470,8 @@
             pltpu.VMEM((HEADS, rows * DK, DV), BF16),
             pltpu.VMEM((ep * CAP, width), BF16),
             pltpu.VMEM((ep * CAP, ff), BF16),
-            pltpu.VMEM((wide, wide), BF16),
-            pltpu.VMEM((wide, wide), BF16),
+            pltpu.VMEM((wide // 2, wide // 2), BF16),
+            pltpu.VMEM((wide // 2, wide // 2), BF16),
             pltpu.SemaphoreType.DMA((17,)),
             pltpu.SemaphoreType.DMA((5,)),
             pltpu.SemaphoreType.DMA((5,)),

time: 72 us -> 71 us (0.986)
  Pallas kernels: 71.2 us -> 70.2 us
    pallas_call x1, Pallas kernels: 68.8 us -> 67.8 us  [per_device(): pl.pallas_call(functools.partial(kernel, ep), out_shape=(jax.ShapeDtypeSt...]
where the time goes in v6:
time: 71 us; the launch traced here: 70.9 us
  Pallas kernels  70.2 us (99%)
    pallas_call x1, Pallas kernels, per_device(): pl.pallas_call(functools.partial(kernel, ep), out_shape=(jax.ShapeDtypeSt...  67.8 us
    pallas_call x1, Pallas kernels, per_device(): pl.pallas_call(finish, out_shape=(jax.ShapeDtypeStruct((rows, width), BF1...  2.41 us

profile of v6, /device:TPU:69, one launch (start us, length us, event | category | flops | bytes accessed | tf_op | source)
XLA Modules:
  0.0 70.9 jit_solution(2114271475968653607)
XLA Ops:
  0.6 67.8 %layer.1 = (bf16[8,2048]{1,0:T(8,128)(2,1)}, f32[8,8,64,128]{3,2,1,0:T(8,128)}) custom-call(bf16[8,2048]{1,0:T(8,128)(2,1)} %tokens_in.1, f32[1,2048]{1,0:T(1,128)} %bitcast.8, bf16[32,2048]{1,0:T(8,128)(2,1)} %bitcast.7, bf16[32,512]{1,0:T(8,128)(2,1)} %w_du_in.1, f32[1,512]{1,0:T(1,128)} %bitcast.10, f32[1,128]{1,0:T(1,128)} %bitcast.13, ...), custom_call_target="tpu_custom_call" | custom-call | tf_op jit(solution)/shard_map/layer/pallas_call | solution.py:436
  68.4 2.4 %finish.1 = (bf16[8,2048]{1,0:T(8,128)(2,1)}, f32[8,8,64,128]{3,2,1,0:T(8,128)}) custom-call(bf16[8,2048]{1,0:T(8,128)(2,1)} %get-tuple-element.4.out_in, f32[8,8,64,128]{3,2,1,0:T(8,128)} %get-tuple-element.5.state_in), custom_call_target="tpu_custom_call" | custom-call | tf_op jit(solution)/shard_map/finish/pallas_call | solution.py:502

commit v7 on v6

--- a/solution.py
+++ b/solution.py
@@ -174,7 +174,7 @@
     for n in (1, -1):
         for cc in range(2):
             copy(own_w.at[cc], wbuf.at[2 * (1 - n) + core], 1, dev(z + n, cc)).start()
-    copy(own_w.at[1 - core], wbuf.at[2 + core], 1, dev(z, 1 - core)).start()
+    copy(own_w.at[1 - core], wbuf.at[2 + core], 5, dev(z, 1 - core)).start()
 
     wbuf[2 + core] = own_w[core]
     for cc in range(2):
@@ -239,13 +239,15 @@
         pltpu.make_async_copy(
             xbuf.at[pl.ds(0, units)], xbuf.at[pl.ds(0, units)], recv_sems.at[0]
         ).wait()
-    with jax.named_scope("weights_wait"):
-        pltpu.make_async_copy(
-            wbuf.at[pl.ds(0, 5)], wbuf.at[pl.ds(0, 5)], recv_sems.at[1]
-        ).wait()
+    pltpu.make_async_copy(wbuf.at[0], wbuf.at[0], recv_sems.at[5]).wait()
     cols = wbuf.shape[2]
     part = None
-    for n in range(3):
+    for n in (1, 0, 2):
+        if n == 0:
+            with jax.named_scope("weights_wait"):
+                pltpu.make_async_copy(
+                    wbuf.at[pl.ds(0, 4)], wbuf.at[pl.ds(0, 4)], recv_sems.at[1]
+                ).wait()
         x = jnp.concatenate(
             [xbuf[3 * i + n].astype(F32) for i in range(chunks)], axis=0
         ).astype(BF16)
@@ -372,7 +374,8 @@
         arrive(rsend, rrecv, 4)
 
     back = rrecv[...].reshape(wide, lanes)
-    mixed = dot(combine_hi, back) + dot(combine_lo, back)
+    both = dot(jnp.concatenate([combine_hi, combine_lo], axis=0), back)
+    mixed = both[:tall] + both[tall:]
     for k in range(kbs):
         at = slice(lanes * k, lanes * (k + 1))
         out[:, at] = (residual[:, at] + mixed[rows * k : rows * (k + 1)]).astype(BF16)
@@ -381,7 +384,8 @@
     pltpu.make_async_copy(
         xbuf.at[pl.ds(0, units)], xbuf.at[pl.ds(0, units)], send_sems.at[0]
     ).wait()
-    pltpu.make_async_copy(wbuf.at[pl.ds(0, 5)], wbuf.at[pl.ds(0, 5)], send_sems.at[1]).wait()
+    pltpu.make_async_copy(wbuf.at[pl.ds(0, 4)], wbuf.at[pl.ds(0, 4)], send_sems.at[1]).wait()
+    pltpu.make_async_copy(wbuf.at[0], wbuf.at[0], send_sems.at[5]).wait()
     pltpu.make_async_copy(psend, rbuf, send_sems.at[2]).wait()
     for src, dst, phase in ((dsend, drecv, 3), (rsend, rrecv, 4)):
         pltpu.make_async_copy(
@@ -473,8 +477,8 @@
             pltpu.VMEM((wide // 2, wide // 2), BF16),
             pltpu.VMEM((wide // 2, wide // 2), BF16),
             pltpu.SemaphoreType.DMA((17,)),
-            pltpu.SemaphoreType.DMA((5,)),
-            pltpu.SemaphoreType.DMA((5,)),
+            pltpu.SemaphoreType.DMA((6,)),
+            pltpu.SemaphoreType.DMA((6,)),
         ],
         compiler_params=pltpu.CompilerParams(
             collective_id=0, has_side_effects=True, vmem_limit_bytes=63_000_000

time: 71 us -> 70.8 us (level)
  no operation moved by 1% of the time
where the time goes in v7:
time: 70.8 us; the launch traced here: 70.7 us
  Pallas kernels  70 us (99%)
    pallas_call x1, Pallas kernels, per_device(): pl.pallas_call(functools.partial(kernel, ep), out_shape=(jax.ShapeDtypeSt...  67.6 us
    pallas_call x1, Pallas kernels, per_device(): pl.pallas_call(finish, out_shape=(jax.ShapeDtypeStruct((rows, width), BF1...  2.41 us

profile of v7, /device:TPU:69, one launch (start us, length us, event | category | flops | bytes accessed | tf_op | source)
XLA Modules:
  0.0 70.7 jit_solution(15259528417417090706)
XLA Ops:
  0.6 67.6 %layer.1 = (bf16[8,2048]{1,0:T(8,128)(2,1)}, f32[8,8,64,128]{3,2,1,0:T(8,128)}) custom-call(bf16[8,2048]{1,0:T(8,128)(2,1)} %tokens_in.1, f32[1,2048]{1,0:T(1,128)} %bitcast.8, bf16[32,2048]{1,0:T(8,128)(2,1)} %bitcast.7, bf16[32,512]{1,0:T(8,128)(2,1)} %w_du_in.1, f32[1,512]{1,0:T(1,128)} %bitcast.10, f32[1,128]{1,0:T(1,128)} %bitcast.13, ...), custom_call_target="tpu_custom_call" | custom-call | tf_op jit(solution)/shard_map/layer/pallas_call | solution.py:440
  68.2 2.4 %finish.1 = (bf16[8,2048]{1,0:T(8,128)(2,1)}, f32[8,8,64,128]{3,2,1,0:T(8,128)}) custom-call(bf16[8,2048]{1,0:T(8,128)(2,1)} %get-tuple-element.4.out_in, f32[8,8,64,128]{3,2,1,0:T(8,128)} %get-tuple-element.5.state_in), custom_call_target="tpu_custom_call" | custom-call | tf_op jit(solution)/shard_map/finish/pallas_call | solution.py:506
